TPU v7x, 32 devices: a whole 2x2x4 slice. The times are simulated.
32 devices in a mesh: sp: 8 (over z, y), tp: 4 (over x, core).
Axes of the slice: x: 2, y: 2, z: 4, core: 2. Of those that a mesh axis runs over, the one named last changes fastest.
Arguments:
- tokens: bfloat16 [8192, 2048], P('sp', 'tp'), may hold values from -16 to 16
- mix_gain: float32 [2048], replicated, may hold values from 0.1 to 1.9
- query_weight: bfloat16 [2048, 1024], P(None, 'tp'), may hold values from -0.125 to 0.125
- key_weight: bfloat16 [2048, 1024], P(None, 'tp'), may hold values from -0.125 to 0.125
- value_weight: bfloat16 [2048, 1024], P(None, 'tp'), may hold values from -0.125 to 0.125
- outer_gate_weight: bfloat16 [2048, 1024], P(None, 'tp'), may hold values from -0.125 to 0.125
- inner_gate_weight: bfloat16 [2048, 1024], P(None, 'tp'), may hold values from -0.125 to 0.125
- conv_input_weight: bfloat16 [2048, 1024], P(None, 'tp'), may hold values from -0.125 to 0.125
- query_gain: float32 [64], replicated, may hold values from 0.6 to 10
- key_gain: float32 [64], replicated, may hold values from 0.6 to 10
- gate_totals: float32 [8192, 16], P('sp', 'tp'), may hold values from -2048 to 0, as said below
- conv_taps: float32 [3, 1024], P(None, 'tp'), may hold values from -3 to 3
- attn_out_gain: float32 [1024], P('tp'), may hold values from 0.1 to 1.9
- conv_out_gain: float32 [1024], P('tp'), may hold values from 0.1 to 1.9
- attn_out_weight: bfloat16 [1024, 2048], P('tp'), may hold values from -0.125 to 0.125
- conv_out_weight: bfloat16 [1024, 2048], P('tp'), may hold values from -0.125 to 0.125
Outputs:
- mixed: bfloat16 [8192, 2048], P(('sp', 'tp'))
Inputs may be any that keep to these rules, and one draw needn't show every extreme that they name: `gate_totals`: in every head the values never rise from one position to the next.
All inputs are finite; a program needn't handle non-finite values.
Results may differ from a plain program's by a relative error of at most 0.015.
The roundings to bfloat16 on the way count: a program that leaves them out, or rounds other values in their place, can miss the bound.
Values may be sent and summed in bfloat16 or wider, within the bound.
A program may use at most 64 MiB of HBM per device.

v0:
```python
import functools

import jax
import jax.numpy as jnp
from jax import lax
from jax.experimental import pallas as pl
from jax.experimental.pallas import tpu as pltpu
from jax.sharding import PartitionSpec as P

NORM_EPSILON = 1e-06
MESH = pl.DeviceIdType.MESH
CORES = 2
LANES = 128
VMEM = pltpu.VMEM


def greet(devices):
    barrier = pltpu.get_barrier_semaphore()
    for sp, tp in devices:
        pl.semaphore_signal(barrier, inc=1, device_id=(sp, tp), device_id_type=MESH)
    pl.semaphore_wait(barrier, len(devices))


def mesh_copy(src, dst, send, recv, device):
    return pltpu.make_async_remote_copy(
        src, dst, send, recv, device_id=device, device_id_type=MESH
    )


def front_kernel(
    plan, tokens_ref, mix_ref, query_gain_ref, key_gain_ref, taps_ref, conv_gain_ref, side_ref, *refs
):
    sp_count, tp_count, head_count, head_dim, chunk = plan
    query_gain = jnp.concatenate([query_gain_ref[...]] * plan[2], axis=1)
    key_gain = jnp.concatenate([key_gain_ref[...]] * plan[2], axis=1)
    weight_refs = refs[:6]
    kv_out, query_out, side_out, conv_out = refs[6:10]
    (
        weights, gathered, scaled, kv_send, query_send, outer, padded, edge_send, edge_recv,
        weight_sem, own_sem, cross_send, mate_send, tok_pass_send, tok_recv,
        kv_ssem, kv_rsem, query_ssem, query_rsem, side_ssem, side_rsem,
        kv_psem, kv_prsem, query_psem, query_prsem, side_psem, side_prsem, local, edge_sem,
    ) = refs[10:]
    sp = lax.axis_index("sp")
    tp = lax.axis_index("tp")
    core = lax.rem(tp, CORES)
    mate = tp + 1 - 2 * core
    chips = tp_count // CORES
    targets = sp_count // CORES
    share = targets // head_count
    rows, features = tokens_ref.shape
    chunks = rows // chunk
    half = chunk // 2
    width = head_count * head_dim
    order = [chunks - 1] + list(range(chunks - 1))

    loads = [
        pltpu.make_async_copy(ref, weights.at[index], weight_sem.at[index])
        for index, ref in enumerate(weight_refs)
    ]
    for load in loads:
        load.start()
    mine = pltpu.make_async_copy(tokens_ref, gathered.at[tp], own_sem)
    mine.start()
    padded[0:8, :] = jnp.zeros((8, width), jnp.float32)
    greet(
        [(lax.rem(sp + step, sp_count), tp) for step in range(1, sp_count)]
        + [(sp, mate)]
        + [(sp, lax.rem(tp + CORES * step, tp_count)) for step in range(1, chips)]
    )

    def block(number):
        return pl.ds(number * chunk, chunk)

    def to_mate(number):
        return mesh_copy(
            tokens_ref.at[block(number)], gathered.at[tp, block(number)], mate_send.at[number],
            tok_recv.at[tp, number], (sp, mate),
        )

    def across(step, number):
        return mesh_copy(
            tokens_ref.at[block(number)], gathered.at[tp, block(number)],
            cross_send.at[step - 1, number], tok_recv.at[tp, number],
            (sp, lax.rem(tp + CORES * step, tp_count)),
        )

    def token_pass(step, number):
        other = lax.rem(tp + CORES * step, tp_count)
        return mesh_copy(
            gathered.at[other, block(number)], gathered.at[other, block(number)],
            tok_pass_send.at[step - 1, number], tok_recv.at[other, number], (sp, mate),
        )

    def token_arrival(source, number):
        return mesh_copy(
            tokens_ref.at[block(number)], gathered.at[source, block(number)], mate_send.at[number],
            tok_recv.at[source, number], (sp, mate),
        )

    for number in order:
        for step in range(1, chips):
            across(step, number).start()
        to_mate(number).start()

    owner = core == sp // targets

    def target_of(step):
        at = lax.rem(sp + 1 + step, targets)
        return at // share, core * targets + at

    def side_copy(step, head, target):
        return mesh_copy(
            side_ref.at[head], side_out.at[sp], side_ssem.at[step], side_rsem.at[sp], (target, tp)
        )

    def kv_copy(step, number, head, target):
        return mesh_copy(
            kv_send.at[head, block(number)], kv_out.at[sp, block(number)],
            kv_ssem.at[step, number], kv_rsem.at[sp, number], (target, tp),
        )

    def query_copy(step, number, head, target):
        at = pl.ds(number * half, half)
        return mesh_copy(
            query_send.at[head, at], query_out.at[sp, at],
            query_ssem.at[step, number], query_rsem.at[sp, number], (target, tp),
        )

    def kept(number, head):
        at = pl.ds(number * half, half)
        return (
            pltpu.make_async_copy(
                kv_send.at[head, block(number)], kv_out.at[sp, block(number)], local.at[0, number]
            ),
            pltpu.make_async_copy(
                query_send.at[head, at], query_out.at[sp, at], local.at[1, number]
            ),
        )

    def kept_side(head):
        return pltpu.make_async_copy(side_ref.at[head], side_out.at[sp], local.at[2, 0])

    for step in range(targets):
        head, target = target_of(step)

        @pl.when(target != sp)
        def _():
            side_copy(step, head, target).start()

        @pl.when(target == sp)
        def _():
            kept_side(head).start()

    ones_row = lax.broadcasted_iota(jnp.int32, (width, width), 0) // head_dim
    ones_column = lax.broadcasted_iota(jnp.int32, (width, width), 1) // head_dim
    spread = jnp.where(ones_row == ones_column, 1.0 / head_dim, 0.0).astype(jnp.bfloat16)

    def normed(values, gain):
        squares = values * values
        high = squares.astype(jnp.bfloat16)
        low = (squares - high.astype(jnp.float32)).astype(jnp.bfloat16)
        mean = jnp.dot(high, spread, preferred_element_type=jnp.float32)
        mean = mean + jnp.dot(low, spread, preferred_element_type=jnp.float32)
        return values * lax.rsqrt(mean + NORM_EPSILON) * gain

    mine.wait()
    for load in loads:
        load.wait()
    for number in order:
        here = block(number)
        for step in range(1, chips):
            token_arrival(lax.rem(tp + CORES * step, tp_count), number).wait_recv()
            token_pass(step, number).start()
        token_arrival(mate, number).wait_recv()
        for step in range(1, chips):
            token_arrival(lax.rem(mate + CORES * step, tp_count), number).wait_recv()
        total = jnp.zeros((chunk, 1), jnp.float32)
        for source in range(tp_count):
            part = gathered[source, here, :].astype(jnp.float32)
            at = slice(source * features, (source + 1) * features)
            total = total + jnp.sum(part * part, axis=1, keepdims=True)
            scaled[:, at] = (part * mix_ref[:, at]).astype(jnp.bfloat16)
        row_scale = lax.rsqrt(total / (tp_count * features) + NORM_EPSILON)

        def project(index):
            product = jnp.dot(scaled[...], weights[index], preferred_element_type=jnp.float32)
            return product * row_scale

        keys = normed(project(1), key_gain).astype(jnp.bfloat16)
        values = project(2).astype(jnp.bfloat16)
        queries = normed(project(0), query_gain).astype(jnp.bfloat16)
        queries = (queries.astype(jnp.float32) * head_dim ** (-0.5)).astype(jnp.bfloat16)
        for head in range(head_count):
            at = slice(head * head_dim, (head + 1) * head_dim)
            kv_send[head, here, :] = jnp.concatenate([keys[:, at], values[:, at]], axis=1)
            query_send[head, pl.ds(number * half, half), :] = jnp.concatenate(
                [queries[:half, at], queries[half:, at]], axis=1
            )
        for step in range(targets):
            head, target = target_of(step)

            @pl.when(target != sp)
            def _():
                kv_copy(step, number, head, target).start()
                query_copy(step, number, head, target).start()

            @pl.when(target == sp)
            def _():
                for copy in kept(number, head):
                    copy.start()

        outer[here, :] = project(3)
        gated = (project(4) * project(5)).astype(jnp.bfloat16)
        padded[pl.ds(8 + number * chunk, chunk), :] = gated.astype(jnp.float32)
        if number == chunks - 1:
            edge_send[...] = gated[chunk - 16 :, :]

            @pl.when(sp < sp_count - 1)
            def _():
                mesh_copy(
                    edge_send, edge_recv, edge_sem.at[0], edge_sem.at[1],
                    (lax.rem(sp + 1, sp_count), tp),
                ).start()

    edge = mesh_copy(
        edge_send, edge_recv, edge_sem.at[0], edge_sem.at[1], (lax.rem(sp + 1, sp_count), tp)
    )

    @pl.when(sp > 0)
    def _():
        edge.wait_recv()
        padded[0:8, :] = edge_recv[8:16, :].astype(jnp.float32)

    taps = taps_ref.shape[0]
    for number in range(chunks):
        convolved = jnp.zeros((chunk, width), jnp.float32)
        for tap in range(taps):
            at = pl.ds(8 - taps + 1 + tap + number * chunk, chunk)
            convolved = convolved + taps_ref[tap : tap + 1, :] * padded[at, :]
        conv_out[block(number), :] = normed(
            outer[block(number), :] * convolved, conv_gain_ref[...]
        ).astype(jnp.bfloat16)

    def kv_pass(source, number):
        return mesh_copy(
            kv_out.at[source, block(number)], kv_out.at[source, block(number)],
            kv_psem.at[source, number], kv_prsem.at[source, number], (sp, mate),
        )

    def query_pass(source, number):
        at = pl.ds(number * half, half)
        return mesh_copy(
            query_out.at[source, at], query_out.at[source, at],
            query_psem.at[source, number], query_prsem.at[source, number], (sp, mate),
        )

    def side_pass(source):
        return mesh_copy(
            side_out.at[source], side_out.at[source], side_psem.at[source], side_prsem.at[source],
            (sp, mate),
        )

    sources = [lax.rem(sp + step, sp_count) for step in range(sp_count)]

    @pl.when(owner)
    def _():
        for step, source in enumerate(sources):
            if step == 0:
                kept_side(0).wait()
            else:
                mesh_copy(
                    side_ref.at[0], side_out.at[source], side_ssem.at[0], side_rsem.at[source],
                    (sp, mate),
                ).wait_recv()
            side_pass(source).start()
        for number in order:
            at = pl.ds(number * half, half)
            for step, source in enumerate(sources):
                if step == 0:
                    for copy in kept(number, 0):
                        copy.wait()
                else:
                    mesh_copy(
                        kv_send.at[0, block(number)], kv_out.at[source, block(number)],
                        kv_ssem.at[0, number], kv_rsem.at[source, number], (sp, mate),
                    ).wait_recv()
                    mesh_copy(
                        query_send.at[0, at], query_out.at[source, at],
                        query_ssem.at[0, number], query_rsem.at[source, number], (sp, mate),
                    ).wait_recv()
                kv_pass(source, number).start()
                query_pass(source, number).start()
        for source in sources:
            side_pass(source).wait_send()
            for number in order:
                kv_pass(source, number).wait_send()
                query_pass(source, number).wait_send()

    @pl.when(jnp.logical_not(owner))
    def _():
        for source in sources:
            side_pass(source).wait_recv()
            for number in order:
                kv_pass(source, number).wait_recv()
                query_pass(source, number).wait_recv()

    for step in range(targets):
        head, target = target_of(step)

        @pl.when(target != sp)
        def _():
            side_copy(step, head, target).wait_send()
            for number in order:
                kv_copy(step, number, head, target).wait_send()
                query_copy(step, number, head, target).wait_send()

    for number in order:
        to_mate(number).wait_send()
        for step in range(1, chips):
            across(step, number).wait_send()
            token_pass(step, number).wait_send()

    @pl.when(sp < sp_count - 1)
    def _():
        edge.wait_send()


def front(tokens, mix_gain, query_gain, key_gain, taps, conv_gain, sides, weights, head_dim, piece):
    sp_count = lax.axis_size("sp")
    tp_count = lax.axis_size("tp")
    rows, features = tokens.shape
    width = weights[0].shape[1]
    heads = width // head_dim
    chunk = min(256, piece)
    chunks = rows // chunk
    chips = tp_count // CORES
    targets = sp_count // CORES
    bf16 = jnp.bfloat16
    dma = pltpu.SemaphoreType.DMA
    across = (max(chips - 1, 1), chunks)
    vmem = pl.BlockSpec(memory_space=VMEM)
    return pl.pallas_call(
        functools.partial(front_kernel, (sp_count, tp_count, heads, head_dim, chunk)),
        out_shape=(
            jax.ShapeDtypeStruct((sp_count, rows, LANES), bf16),
            jax.ShapeDtypeStruct((sp_count, rows // 2, LANES), bf16),
            jax.ShapeDtypeStruct((sp_count,) + sides.shape[1:], sides.dtype),
            jax.ShapeDtypeStruct((rows, width), bf16),
        ),
        in_specs=[vmem] * 7 + [pl.BlockSpec(memory_space=pl.ANY)] * 6,
        out_specs=(vmem,) * 4,
        scratch_shapes=[
            VMEM((6,) + weights[0].shape, bf16),
            VMEM((tp_count, rows, features), bf16),
            VMEM((chunk, tp_count * features), bf16),
            VMEM((heads, rows, LANES), bf16),
            VMEM((heads, rows // 2, LANES), bf16),
            VMEM((rows, width), jnp.float32),
            VMEM((rows + 8, width), jnp.float32),
            VMEM((16, width), bf16),
            VMEM((16, width), bf16),
            dma((6,)), dma, dma(across), dma((chunks,)), dma(across), dma((tp_count, chunks)),
            dma((targets, chunks)), dma((sp_count, chunks)),
            dma((targets, chunks)), dma((sp_count, chunks)),
            dma((targets,)), dma((sp_count,)),
            dma((sp_count, chunks)), dma((sp_count, chunks)),
            dma((sp_count, chunks)), dma((sp_count, chunks)),
            dma((sp_count,)), dma((sp_count,)),
            dma((3, chunks)), dma((2,)),
        ],
        compiler_params=pltpu.CompilerParams(
            collective_id=0, has_side_effects=True, vmem_limit_bytes=56 * 1024 * 1024
        ),
    )(tokens, mix_gain, query_gain, key_gain, taps, conv_gain, sides, *weights)


def rear_kernel(
    plan, query_ref, kv_ref, side_ref, conv_ref, attn_weight, conv_weight, out_ref, done, landed,
    attn, partial, keep, mate_out, mate_in, link_out, link_in, send, recv, local, mate_ssem,
    mate_rsem, link_ssem, link_rsem
):
    sp_count, tp_count, head_dim, piece, sub = plan
    sp = lax.axis_index("sp")
    tp = lax.axis_index("tp")
    core = lax.rem(tp, CORES)
    mate = tp + 1 - 2 * core
    chips = tp_count // CORES
    first = tp - core
    targets = sp_count // CORES
    rows, width = conv_ref.shape
    pieces = rows // piece
    share = pieces // CORES
    block_rows = rows // tp_count
    chunk = min(256, piece)
    half = chunk // 2
    tile = piece // 2
    span = 256
    phases = 2
    subs = block_rows // phases // sub
    greet(
        [
            (lax.rem(sp + step, sp_count), first + lax.rem(core + other, CORES))
            for step in range(sp_count)
            for other in range(CORES)
            if step or other
        ]
        + [(sp, lax.rem(tp + CORES * step, tp_count)) for step in range(1, chips)]
    )
    home = sp // targets
    slot = lax.rem(sp, targets) * CORES + core
    home_here = home == core
    place_here = lax.rem(sp, share) * CORES + core
    low = lax.broadcasted_iota(jnp.int32, (half, LANES), 1) < head_dim
    gain = side_ref[0, rows // LANES : rows // LANES + 1, :head_dim]

    def away(phase, source):
        return mesh_copy(
            done.at[phase, source], landed.at[phase, slot], send.at[phase, source],
            recv.at[phase, slot], (source, first + home),
        )

    def stay(phase, source, index):
        return pltpu.make_async_copy(
            done.at[phase, source], landed.at[phase, index], local.at[phase]
        )

    def queries_of(phase, source, spot):
        begin = pl.multiple_of(spot * tile, half)
        parts = []
        for number in range(piece // chunk):
            pair = query_ref[source, pl.ds(begin + number * half, half), :].astype(jnp.float32)
            if phase:
                pair = pltpu.roll(pair, head_dim, 1)
            parts.append(jnp.where(low, pair, 0.0))
        return jnp.concatenate(parts, axis=0).astype(jnp.bfloat16)

    def fold(phase, source, queries, carried, spot=None):
        top, total = carried
        new_top = top
        scores = []
        for start in range(0, rows, span):
            gates = side_ref[source, start // LANES : (start + span) // LANES, :]
            gate_row = jnp.concatenate(
                [gates[row : row + 1, :] for row in range(span // LANES)], axis=1
            )
            part = lax.dot_general(
                queries, kv_ref[source, start : start + span, :],
                (((1,), (1,)), ((), ())), preferred_element_type=jnp.float32,
            ) - gate_row
            if spot is not None:
                row = lax.broadcasted_iota(jnp.int32, part.shape, 0)
                row = row // half * chunk + lax.rem(row, half) + phase * half + spot * piece
                column = lax.broadcasted_iota(jnp.int32, part.shape, 1) + start
                part = jnp.where(column <= row, part, -jnp.inf)
            new_top = jnp.maximum(new_top, jnp.max(part, axis=1, keepdims=True))
            scores.append(part)
        total = total * jnp.exp(top - new_top)
        for index, part in enumerate(scores):
            weights = jnp.exp(part - new_top).astype(jnp.bfloat16)
            total = total + jnp.dot(
                weights, kv_ref[source, index * span : (index + 1) * span, :],
                preferred_element_type=jnp.float32,
            )
        return new_top, total

    def finish(phase, source, carried):
        attended = carried[1][:, head_dim:]
        scale = lax.rsqrt(jnp.mean(attended * attended, axis=1, keepdims=True) + NORM_EPSILON)
        mixed = (attended * scale * gain).astype(jnp.bfloat16)
        done[phase, source, :, :] = jnp.concatenate(
            [mixed[: tile // 2], mixed[tile // 2 :]], axis=1
        )
        stays = jnp.logical_and(source == sp, home_here)

        @pl.when(stays)
        def _():
            stay(phase, source, slot).start()

        @pl.when(jnp.logical_not(stays))
        def _():
            away(phase, source).start()

    def attend(phase):
        def pair_of_sources(pair, _):
            even, odd = 2 * pair, 2 * pair + 1
            even_spot, odd_spot = place_here, pieces - 1 - place_here
            even_queries = queries_of(phase, even, even_spot)
            odd_queries = queries_of(phase, odd, odd_spot)
            empty = (
                jnp.full((tile, 1), -1e30, jnp.float32),
                jnp.zeros((tile, LANES), jnp.float32),
            )

            def both(source, carried):
                return (
                    fold(phase, source, even_queries, carried[0]),
                    fold(phase, source, odd_queries, carried[1]),
                )

            even_state, odd_state = lax.fori_loop(0, even, both, (empty, empty))
            odd_state = fold(phase, even, odd_queries, odd_state)
            even_state = fold(phase, even, even_queries, even_state, even_spot)
            odd_state = fold(phase, odd, odd_queries, odd_state, odd_spot)
            finish(phase, even, even_state)
            finish(phase, odd, odd_state)
            return 0

        lax.fori_loop(0, sp_count // 2, pair_of_sources, 0)

    def arrive(phase):
        for index in range(targets * CORES):
            giver = core * targets + index // CORES
            here = jnp.logical_and(giver == sp, core == index % CORES)

            @pl.when(here)
            def _():
                stay(phase, 0, index).wait()

            @pl.when(jnp.logical_not(here))
            def _():
                mesh_copy(
                    done.at[phase, 0], landed.at[phase, index], send.at[phase, 0],
                    recv.at[phase, index], (sp, mate),
                ).wait_recv()

            head = index // (share * CORES)
            place = index % (share * CORES)
            spot = jnp.where(lax.rem(sp, 2) == 0, place, pieces - 1 - place)
            lanes = slice(head * head_dim, (head + 1) * head_dim)
            for side, at in enumerate((0, tile // 2)):
                offset = at // half * chunk + phase * half + at % half
                start = pl.multiple_of(spot * piece + offset, tile // 2)
                attn[pl.ds(start, tile // 2), lanes] = landed[
                    phase, index, :, side * head_dim : (side + 1) * head_dim
                ]

    def product(block, number):
        at = pl.ds(pl.multiple_of(block * block_rows + number * sub, sub), sub)
        return partial[at, :] + jnp.dot(
            attn[at, :], attn_weight[...], preferred_element_type=jnp.float32
        )

    def within(number):
        return pl.ds(number * sub, sub)

    def to_mate(step, number):
        at = within(number)
        return mesh_copy(
            mate_out.at[step, at], mate_in.at[step, at], mate_ssem.at[step, number],
            mate_rsem.at[step, number], (sp, mate),
        )

    def across(step, number):
        at = within(number)
        return mesh_copy(
            link_out.at[step - 1, at], link_in.at[step - 1, at], link_ssem.at[step - 1, number],
            link_rsem.at[step - 1, number], (sp, lax.rem(tp + CORES * step, tp_count)),
        )

    def joined(step, number):
        at = within(number)
        to_mate(step, number).wait_recv()
        total = keep[step, at, :] + mate_in[step, at, :].astype(jnp.float32)
        link_out[step - 1, at, :] = total.astype(jnp.bfloat16)
        across(step, number).start()

    def spread(phase):
        waiting = []
        for step in list(range(1, chips)) + [0]:
            for number in range(phase * subs, (phase + 1) * subs):
                at = within(number)
                theirs = lax.rem(mate + CORES * step, tp_count)
                ours = lax.rem(tp + CORES * step, tp_count)
                mate_out[step, at, :] = product(theirs, number).astype(jnp.bfloat16)
                to_mate(step, number).start()
                keep[step, at, :] = product(ours, number)
                if waiting:
                    joined(*waiting.pop())
                if step:
                    waiting.append((step, number))

    def settle(phase):
        for number in range(phase * subs, (phase + 1) * subs):
            at = within(number)
            to_mate(0, number).wait_recv()
            total = keep[0, at, :] + mate_in[0, at, :].astype(jnp.float32)
            for step in range(1, chips):
                across(step, number).wait_recv()
                total = total + link_in[step - 1, at, :].astype(jnp.float32)
            out_ref[at, :] = total.astype(jnp.bfloat16)

    attend(0)
    for number in range(tp_count):
        at = pl.ds(number * block_rows, block_rows)
        partial[at, :] = jnp.dot(
            conv_ref[at, :], conv_weight[...], preferred_element_type=jnp.float32
        )
    arrive(0)
    spread(0)
    attend(1)
    settle(0)
    arrive(1)
    spread(1)
    settle(1)
    for step in range(chips):
        for number in range(phases * subs):
            to_mate(step, number).wait_send()
            if step:
                across(step, number).wait_send()
    for phase in range(phases):
        for step in range(1, sp_count):
            away(phase, lax.rem(sp + step, sp_count)).wait_send()

        @pl.when(jnp.logical_not(home_here))
        def _():
            away(phase, sp).wait_send()


def rear(queries, kv, sides, conv_mixed, attn_weight, conv_weight, head_dim, piece):
    sp_count = lax.axis_size("sp")
    tp_count = lax.axis_size("tp")
    chips = tp_count // CORES
    rows, width = conv_mixed.shape
    features = attn_weight.shape[1]
    block_rows = rows // tp_count
    sub = min(64, block_rows // 2)
    subs = block_rows // sub
    links = max(chips - 1, 1)
    bf16 = jnp.bfloat16
    dma = pltpu.SemaphoreType.DMA
    vmem = pl.BlockSpec(memory_space=VMEM)
    return pl.pallas_call(
        functools.partial(rear_kernel, (sp_count, tp_count, head_dim, piece, sub)),
        out_shape=jax.ShapeDtypeStruct((block_rows, features), bf16),
        in_specs=[vmem] * 6,
        out_specs=vmem,
        scratch_shapes=[
            VMEM((2, sp_count, piece // 4, LANES), bf16),
            VMEM((2, sp_count, piece // 4, LANES), bf16),
            VMEM((rows, width), bf16),
            VMEM((rows, features), jnp.float32),
            VMEM((chips, block_rows, features), jnp.float32),
            VMEM((chips, block_rows, features), bf16),
            VMEM((chips, block_rows, features), bf16),
            VMEM((links, block_rows, features), bf16),
            VMEM((links, block_rows, features), bf16),
            dma((2, sp_count)), dma((2, sp_count)), dma((2,)),
            dma((chips, subs)), dma((chips, subs)), dma((links, subs)), dma((links, subs)),
        ],
        compiler_params=pltpu.CompilerParams(
            collective_id=1, has_side_effects=True, vmem_limit_bytes=56 * 1024 * 1024
        ),
    )(queries, kv, sides, conv_mixed, attn_weight, conv_weight)


def per_device(
    tokens,
    mix_gain,
    query_weight,
    key_weight,
    value_weight,
    outer_gate_weight,
    inner_gate_weight,
    conv_input_weight,
    query_gain,
    key_gain,
    gate_totals,
    conv_taps,
    attn_out_gain,
    conv_out_gain,
    attn_out_weight,
    conv_out_weight,
):
    rows = tokens.shape[0]
    head_dim = query_gain.shape[0]
    width = query_weight.shape[1]
    heads = width // head_dim
    sp_count = lax.axis_size("sp")
    share = sp_count // CORES // heads
    pieces = CORES * share
    piece = rows // pieces
    gate_rows = gate_totals.T.reshape(heads, rows // LANES, LANES)
    gain_rows = jnp.pad(
        attn_out_gain.reshape(heads, 1, head_dim), ((0, 0), (0, 7), (0, LANES - head_dim))
    )
    sides = jnp.concatenate([gate_rows, gain_rows], axis=1)
    kv, queries, sides, conv_mixed = front(
        tokens,
        mix_gain.reshape(1, -1),
        query_gain.reshape(1, -1),
        key_gain.reshape(1, -1),
        conv_taps,
        conv_out_gain.reshape(1, -1),
        sides,
        (
            query_weight,
            key_weight,
            value_weight,
            outer_gate_weight,
            inner_gate_weight,
            conv_input_weight,
        ),
        head_dim,
        piece,
    )
    return rear(
        queries, kv, sides, conv_mixed, attn_out_weight, conv_out_weight, head_dim, piece
    )


def solution(mesh):
    placed = (
        P("sp", "tp"),
        P(),
        P(None, "tp"),
        P(None, "tp"),
        P(None, "tp"),
        P(None, "tp"),
        P(None, "tp"),
        P(None, "tp"),
        P(),
        P(),
        P("sp", "tp"),
        P(None, "tp"),
        P("tp"),
        P("tp"),
        P("tp", None),
        P("tp", None),
    )
    return jax.shard_map(
        per_device, mesh=mesh, in_specs=placed, out_specs=P(("sp", "tp"), None), check_vma=False
    )
```

profile of v0, /device:TPU:0, one launch (start us, length us, event | category | flops | bytes accessed | tf_op | source)
XLA Modules:
  0.0 133.2 jit_solution(15007771836863578959)
XLA Ops:
  0.0 0.8 reshape.23
  0.8 0.7 copy.19
  1.5 0.6 select_maximum_fusion.side_ref
  2.1 59.7 %shard_map.154 = (bf16[8,1024,128]{2,1,0:T(8,128)(2,1)}, bf16[8,512,128]{2,1,0:T(8,128)(2,1)}, f32[8,16,128]{2,1,0:T(8,128)}, bf16[1024,256]{1,0:T(8,128)(2,1)}) custom-call(bf16[1024,512]{1,0:T(8,128)(2,1)} %tokens_ref.1, f32[1,2048]{1,0:T(1,128)} %bitcast.11, f32[1,64]{1,0:T(1,128)} %bitcast.13, f32[1,64]{1,0:T(1,128)} %bitcast.14, f32[3,256]{1,0:T(4,128)} %taps_ref.1, ...), custom_call_target="tpu_custom_call" | custom-call | tf_op jit(solution)/shard_map/pallas_call | solution.py:343
  61.8 69.1 %shard_map.155 = bf16[256,2048]{1,0:T(8,128)(2,1)} custom-call(bf16[8,512,128]{2,1,0:T(8,128)(2,1)} %get-tuple-element.9.query_ref, bf16[8,1024,128]{2,1,0:T(8,128)(2,1)} %get-tuple-element.10.kv_ref, f32[8,16,128]{2,1,0:T(8,128)} %get-tuple-element.11.side_ref, bf16[1024,256]{1,0:T(8,128)(2,1)} %get-tuple-element.12.conv_ref, ...), custom_call_target="tpu_custom_call" | custom-call | tf_op jit(solution)/shard_map/pallas_call | solution.py:633
  130.9 2.3 %copy.21 = bf16[256,2048]{1,0:T(8,128)(2,1)} copy(bf16[256,2048]{1,0:T(8,128)(2,1)} %shard_map.155) | data formatting | bytes 2097152
where the time goes:
time: 135 us; the launch traced here: 133 us
  Pallas kernels  129 us (96%)
  local copies, waits for them, and re-layouts  3.78 us (3%)
    pallas_call x1, Pallas kernels, rear(): pl.pallas_call(functools.partial(rear_kernel, (sp_count, tp_count, head_d...  69.1 us
    pallas_call x1, Pallas kernels, front(): pl.pallas_call(functools.partial(front_kernel, (sp_count, tp_count, heads...  59.7 us
    unnamed x2, local copies, waits for them, and re-layouts  3.02 us

commit v1 on v0

--- a/solution.py
+++ b/solution.py
@@ -188,15 +188,29 @@
             return product * row_scale
 
         keys = normed(project(1), key_gain).astype(jnp.bfloat16)
-        values = project(2).astype(jnp.bfloat16)
+        values = project(2)
         queries = normed(project(0), query_gain).astype(jnp.bfloat16)
-        queries = (queries.astype(jnp.float32) * head_dim ** (-0.5)).astype(jnp.bfloat16)
+        queries = queries.astype(jnp.float32) * head_dim ** (-0.5)
         for head in range(head_count):
             at = slice(head * head_dim, (head + 1) * head_dim)
-            kv_send[head, here, :] = jnp.concatenate([keys[:, at], values[:, at]], axis=1)
-            query_send[head, pl.ds(number * half, half), :] = jnp.concatenate(
-                [queries[:half, at], queries[half:, at]], axis=1
+            kv_send[head, pl.ds(number * chunk, half), :] = jnp.concatenate(
+                [keys[:half, at], keys[half:, at]], axis=1
             )
+        for side in range(2):
+            rows_of = slice(side * half, (side + 1) * half)
+            for first in range(0, width, LANES):
+                at = slice(first, first + LANES)
+                flipped_values = values[rows_of, at].T.astype(jnp.bfloat16)
+                flipped_queries = queries[rows_of, at].T.astype(jnp.bfloat16)
+                for inner in range(LANES // head_dim):
+                    head = first // head_dim + inner
+                    piece_of = slice(inner * head_dim, (inner + 1) * head_dim)
+                    kv_send[
+                        head, pl.ds(number * chunk + half + side * head_dim, head_dim), :
+                    ] = flipped_values[piece_of]
+                    query_send[
+                        head, pl.ds(number * half + side * head_dim, head_dim), :
+                    ] = flipped_queries[piece_of]
         for step in range(targets):
             head, target = target_of(step)
 
@@ -332,7 +346,7 @@
     rows, features = tokens.shape
     width = weights[0].shape[1]
     heads = width // head_dim
-    chunk = min(256, piece)
+    chunk = 2 * LANES
     chunks = rows // chunk
     chips = tp_count // CORES
     targets = sp_count // CORES
@@ -377,7 +391,7 @@
 
 def rear_kernel(
     plan, query_ref, kv_ref, side_ref, conv_ref, attn_weight, conv_weight, out_ref, done, landed,
-    attn, partial, keep, mate_out, mate_in, link_out, link_in, send, recv, local, mate_ssem,
+    rhs, gates, scores_a, scores_b, flipped, attn, partial, keep, mate_out, mate_in, link_out, link_in, send, recv, local, mate_ssem,
     mate_rsem, link_ssem, link_rsem
 ):
     sp_count, tp_count, head_dim, piece, sub = plan
@@ -392,11 +406,12 @@
     pieces = rows // piece
     share = pieces // CORES
     block_rows = rows // tp_count
-    chunk = min(256, piece)
-    half = chunk // 2
-    tile = piece // 2
+    half = LANES
+    chunk = 2 * half
+    phases = min(2, piece // half)
+    tile = piece // phases
+    slabs = piece // half
     span = 256
-    phases = 2
     subs = block_rows // phases // sub
     greet(
         [
@@ -411,8 +426,30 @@
     slot = lax.rem(sp, targets) * CORES + core
     home_here = home == core
     place_here = lax.rem(sp, share) * CORES + core
-    low = lax.broadcasted_iota(jnp.int32, (half, LANES), 1) < head_dim
-    gain = side_ref[0, rows // LANES : rows // LANES + 1, :head_dim]
+    bf16 = jnp.bfloat16
+    both_tiles = 2 * tile
+    gain_tile = jnp.broadcast_to(side_ref[0, rows // LANES : rows // LANES + 1, :], (LANES, LANES))
+    gain = gain_tile.T[:head_dim, 0:1]
+
+    def pieces_of(values):
+        high = values.astype(bf16).astype(jnp.float32)
+        middle = (values - high).astype(bf16).astype(jnp.float32)
+        low = (values - high - middle).astype(bf16).astype(jnp.float32)
+        return high, middle, low
+
+    def gate_columns(source, _):
+        cuts = pieces_of(-side_ref[source, : rows // LANES, :])
+        for number in range(rows // chunk):
+            lines = [
+                cut[2 * number + side : 2 * number + side + 1, :] for side in range(2) for cut in cuts
+            ]
+            lines.append(jnp.zeros((LANES - len(lines), LANES), jnp.float32))
+            gates[source, number * half : (number + 1) * half, :] = (
+                jnp.concatenate(lines, axis=0).T.astype(bf16)
+            )
+        return 0
+
+    lax.fori_loop(0, sp_count, gate_columns, 0)
 
     def away(phase, source):
         return mesh_copy(
@@ -426,51 +463,71 @@
         )
 
     def queries_of(phase, source, spot):
-        begin = pl.multiple_of(spot * tile, half)
         parts = []
-        for number in range(piece // chunk):
-            pair = query_ref[source, pl.ds(begin + number * half, half), :].astype(jnp.float32)
-            if phase:
-                pair = pltpu.roll(pair, head_dim, 1)
-            parts.append(jnp.where(low, pair, 0.0))
-        return jnp.concatenate(parts, axis=0).astype(jnp.bfloat16)
-
-    def fold(phase, source, queries, carried, spot=None):
-        top, total = carried
-        new_top = top
-        scores = []
-        for start in range(0, rows, span):
-            gates = side_ref[source, start // LANES : (start + span) // LANES, :]
-            gate_row = jnp.concatenate(
-                [gates[row : row + 1, :] for row in range(span // LANES)], axis=1
+        for slab in range(phase, slabs, phases):
+            begin = pl.multiple_of((spot * slabs + slab) * head_dim, head_dim)
+            parts.append(query_ref[source, pl.ds(begin, head_dim), :])
+        return jnp.concatenate(parts, axis=1)
+
+    def set_queries(phase, even, even_spot, odd, odd_spot):
+        queries = jnp.concatenate(
+            [queries_of(phase, even, even_spot), queries_of(phase, odd, odd_spot)], axis=1
+        )
+        empty = jnp.zeros_like(queries)
+        row = lax.broadcasted_iota(jnp.int32, (LANES, both_tiles), 0)
+        for side in range(2):
+            ones = jnp.logical_and(row >= 3 * side, row < 3 * side + 3)
+            stacked = [queries, empty] if side == 0 else [empty, queries]
+            rhs[side, :, :] = jnp.concatenate(
+                stacked + [jnp.where(ones, 1.0, 0.0).astype(bf16)], axis=0
             )
-            part = lax.dot_general(
-                queries, kv_ref[source, start : start + span, :],
-                (((1,), (1,)), ((), ())), preferred_element_type=jnp.float32,
-            ) - gate_row
-            if spot is not None:
-                row = lax.broadcasted_iota(jnp.int32, part.shape, 0)
-                row = row // half * chunk + lax.rem(row, half) + phase * half + spot * piece
-                column = lax.broadcasted_iota(jnp.int32, part.shape, 1) + start
-                part = jnp.where(column <= row, part, -jnp.inf)
-            new_top = jnp.maximum(new_top, jnp.max(part, axis=1, keepdims=True))
-            scores.append(part)
-        total = total * jnp.exp(top - new_top)
-        for index, part in enumerate(scores):
-            weights = jnp.exp(part - new_top).astype(jnp.bfloat16)
-            total = total + jnp.dot(
-                weights, kv_ref[source, index * span : (index + 1) * span, :],
-                preferred_element_type=jnp.float32,
-            )
-        return new_top, total
-
-    def finish(phase, source, carried):
-        attended = carried[1][:, head_dim:]
-        scale = lax.rsqrt(jnp.mean(attended * attended, axis=1, keepdims=True) + NORM_EPSILON)
-        mixed = (attended * scale * gain).astype(jnp.bfloat16)
-        done[phase, source, :, :] = jnp.concatenate(
-            [mixed[: tile // 2], mixed[tile // 2 :]], axis=1
-        )
+
+    def score(source, side, scores, top, limit):
+        key_rows = jnp.concatenate(
+            [kv_ref[source, pl.ds(number * chunk, half), :] for number in range(rows // chunk)],
+            axis=0,
+        )
+        lhs = jnp.concatenate([key_rows, gates[source, :, :]], axis=1)
+        part = jnp.dot(lhs, rhs[side, :, :], preferred_element_type=jnp.float32)
+        if limit is not None:
+            row = lax.broadcasted_iota(jnp.int32, part.shape, 0)
+            row = row // half * chunk + lax.rem(row, half) + side * half
+            part = jnp.where(row <= limit, part, -jnp.inf)
+        scores[side * (rows // 2) : (side + 1) * (rows // 2), :] = part
+        return jnp.maximum(top, jnp.max(part.reshape(-1, 8, both_tiles), axis=0))
+
+    def blend(source, scores, side, begin, top, total):
+        start = side * (rows // 2) + begin * half
+        weights = jnp.exp(scores[start : start + span, :] - top).astype(bf16)
+        values = jnp.concatenate(
+            [
+                kv_ref[source, pl.ds((begin + index) * chunk + half + side * head_dim, head_dim), :]
+                for index in range(span // half)
+            ],
+            axis=1,
+        )
+        return total + jnp.dot(values, weights, preferred_element_type=jnp.float32)
+
+    def start_top():
+        return jnp.full((8, both_tiles), -jnp.inf, jnp.float32)
+
+    def settle_top(top):
+        return jnp.max(top, axis=0, keepdims=True)
+
+    def advance(old, old_scores, old_top, state, new, new_scores, limit=None):
+        top = jnp.maximum(state[0], old_top)
+        total = state[1] * jnp.exp(state[0] - top)
+        new_top = start_top()
+        for side in range(2):
+            if new is not None:
+                new_top = score(new, side, new_scores, new_top, limit)
+            for begin in range(0, rows // chunk, span // half):
+                total = blend(old, old_scores, side, begin, top, total)
+        return (top, total), settle_top(new_top)
+
+    def finish(phase, source, attended):
+        scale = lax.rsqrt(jnp.mean(attended * attended, axis=0, keepdims=True) + NORM_EPSILON)
+        done[phase, source, :, :] = (attended * scale * gain).astype(bf16)
         stays = jnp.logical_and(source == sp, home_here)
 
         @pl.when(stays)
@@ -485,25 +542,34 @@
         def pair_of_sources(pair, _):
             even, odd = 2 * pair, 2 * pair + 1
             even_spot, odd_spot = place_here, pieces - 1 - place_here
-            even_queries = queries_of(phase, even, even_spot)
-            odd_queries = queries_of(phase, odd, odd_spot)
-            empty = (
-                jnp.full((tile, 1), -1e30, jnp.float32),
-                jnp.zeros((tile, LANES), jnp.float32),
+            set_queries(phase, even, even_spot, odd, odd_spot)
+            column = lax.broadcasted_iota(jnp.int32, (1, both_tiles), 1)
+            inside = lax.rem(column, tile)
+            inside = (inside // half * phases + phase) * half + lax.rem(inside, half)
+            in_even = column < tile
+            even_limit = jnp.where(in_even, inside + even_spot * piece, rows)
+            odd_limit = jnp.where(in_even, -1, inside + odd_spot * piece)
+            state = (
+                jnp.full((1, both_tiles), -1e30, jnp.float32),
+                jnp.zeros((head_dim, both_tiles), jnp.float32),
             )
-
-            def both(source, carried):
-                return (
-                    fold(phase, source, even_queries, carried[0]),
-                    fold(phase, source, odd_queries, carried[1]),
-                )
-
-            even_state, odd_state = lax.fori_loop(0, even, both, (empty, empty))
-            odd_state = fold(phase, even, odd_queries, odd_state)
-            even_state = fold(phase, even, even_queries, even_state, even_spot)
-            odd_state = fold(phase, odd, odd_queries, odd_state, odd_spot)
-            finish(phase, even, even_state)
-            finish(phase, odd, odd_state)
+            top = start_top()
+            for side in range(2):
+                top = score(even, side, scores_a, top, even_limit)
+            state, top = advance(
+                even, scores_a, settle_top(top), state, odd, scores_b, odd_limit
+            )
+
+            def two_sources(step, carried):
+                state, top, last = carried
+                state, top = advance(last, scores_b, top, state, 2 * step, scores_a)
+                state, top = advance(2 * step, scores_a, top, state, 2 * step + 1, scores_b)
+                return state, top, 2 * step + 1
+
+            state, top, last = lax.fori_loop(0, pair, two_sources, (state, top, odd))
+            state, _ = advance(last, scores_b, top, state, None, None)
+            finish(phase, even, state[1][:, :tile])
+            finish(phase, odd, state[1][:, tile:])
             return 0
 
         lax.fori_loop(0, sp_count // 2, pair_of_sources, 0)
@@ -527,13 +593,14 @@
             head = index // (share * CORES)
             place = index % (share * CORES)
             spot = jnp.where(lax.rem(sp, 2) == 0, place, pieces - 1 - place)
-            lanes = slice(head * head_dim, (head + 1) * head_dim)
-            for side, at in enumerate((0, tile // 2)):
-                offset = at // half * chunk + phase * half + at % half
-                start = pl.multiple_of(spot * piece + offset, tile // 2)
-                attn[pl.ds(start, tile // 2), lanes] = landed[
-                    phase, index, :, side * head_dim : (side + 1) * head_dim
+            for inner in range(tile // half):
+                start = pl.multiple_of((spot * slabs + inner * phases + phase) * half, half)
+                flipped[head * head_dim : (head + 1) * head_dim, pl.ds(start, half)] = landed[
+                    phase, index, :, inner * half : (inner + 1) * half
                 ]
+        for slab in range(phase, rows // half, phases):
+            at = slice(slab * half, (slab + 1) * half)
+            attn[at, :] = flipped[:, at].astype(jnp.float32).T.astype(bf16)
 
     def product(block, number):
         at = pl.ds(pl.multiple_of(block * block_rows + number * sub, sub), sub)
@@ -598,11 +665,12 @@
         )
     arrive(0)
     spread(0)
-    attend(1)
-    settle(0)
-    arrive(1)
-    spread(1)
-    settle(1)
+    for phase in range(1, phases):
+        attend(phase)
+        settle(phase - 1)
+        arrive(phase)
+        spread(phase)
+    settle(phases - 1)
     for step in range(chips):
         for number in range(phases * subs):
             to_mate(step, number).wait_send()
@@ -624,6 +692,8 @@
     rows, width = conv_mixed.shape
     features = attn_weight.shape[1]
     block_rows = rows // tp_count
+    phases = min(2, piece // LANES)
+    tile = piece // phases
     sub = min(64, block_rows // 2)
     subs = block_rows // sub
     links = max(chips - 1, 1)
@@ -636,8 +706,13 @@
         in_specs=[vmem] * 6,
         out_specs=vmem,
         scratch_shapes=[
-            VMEM((2, sp_count, piece // 4, LANES), bf16),
-            VMEM((2, sp_count, piece // 4, LANES), bf16),
+            VMEM((phases, sp_count, head_dim, tile), bf16),
+            VMEM((phases, sp_count, head_dim, tile), bf16),
+            VMEM((2, 2 * LANES, 2 * tile), bf16),
+            VMEM((sp_count, rows // 2, LANES), bf16),
+            VMEM((rows, 2 * tile), jnp.float32),
+            VMEM((rows, 2 * tile), jnp.float32),
+            VMEM((width, rows), bf16),
             VMEM((rows, width), bf16),
             VMEM((rows, features), jnp.float32),
             VMEM((chips, block_rows, features), jnp.float32),
@@ -645,7 +720,7 @@
             VMEM((chips, block_rows, features), bf16),
             VMEM((links, block_rows, features), bf16),
             VMEM((links, block_rows, features), bf16),
-            dma((2, sp_count)), dma((2, sp_count)), dma((2,)),
+            dma((phases, sp_count)), dma((phases, sp_count)), dma((phases,)),
             dma((chips, subs)), dma((chips, subs)), dma((links, subs)), dma((links, subs)),
         ],
         compiler_params=pltpu.CompilerParams(

time: 135 us -> 122 us (0.904)
  the two profiles are of different devices: /device:TPU:0 before, /device:TPU:26 now
where the time goes in v1:
time: 122 us; the launch traced here: 121 us
  Pallas kernels  117 us (96%)
  local copies, waits for them, and re-layouts  3.78 us (3%)
    pallas_call x1, Pallas kernels, rear(): pl.pallas_call(functools.partial(rear_kernel, (sp_count, tp_count, head_d...  60.6 us
    pallas_call x1, Pallas kernels, front(): pl.pallas_call(functools.partial(front_kernel, (sp_count, tp_count, heads...  56.5 us
    unnamed x2, local copies, waits for them, and re-layouts  3.02 us

profile of v1, /device:TPU:26, one launch (start us, length us, event | category | flops | bytes accessed | tf_op | source)
XLA Modules:
  0.0 121.5 jit_solution(1574606915678989068)
XLA Ops:
  0.0 0.8 reshape.23
  0.8 0.7 copy.19
  1.5 0.6 select_maximum_fusion.side_ref
  2.1 56.5 %shard_map.154 = (bf16[8,1024,128]{2,1,0:T(8,128)(2,1)}, bf16[8,512,128]{2,1,0:T(8,128)(2,1)}, f32[8,16,128]{2,1,0:T(8,128)}, bf16[1024,256]{1,0:T(8,128)(2,1)}) custom-call(bf16[1024,512]{1,0:T(8,128)(2,1)} %tokens_ref.1, f32[1,2048]{1,0:T(1,128)} %bitcast.11, f32[1,64]{1,0:T(1,128)} %bitcast.13, f32[1,64]{1,0:T(1,128)} %bitcast.14, f32[3,256]{1,0:T(4,128)} %taps_ref.1, ...), custom_call_target="tpu_custom_call" | custom-call | tf_op jit(solution)/shard_map/pallas_call | solution.py:357
  58.6 60.6 %shard_map.155 = bf16[256,2048]{1,0:T(8,128)(2,1)} custom-call(bf16[8,512,128]{2,1,0:T(8,128)(2,1)} %get-tuple-element.9.query_ref, bf16[8,1024,128]{2,1,0:T(8,128)(2,1)} %get-tuple-element.10.kv_ref, f32[8,16,128]{2,1,0:T(8,128)} %get-tuple-element.11.side_ref, bf16[1024,256]{1,0:T(8,128)(2,1)} %get-tuple-element.12.conv_ref, ...), custom_call_target="tpu_custom_call" | custom-call | tf_op jit(solution)/shard_map/pallas_call | solution.py:703
  119.2 2.3 %copy.21 = bf16[256,2048]{1,0:T(8,128)(2,1)} copy(bf16[256,2048]{1,0:T(8,128)(2,1)} %shard_map.155) | data formatting | bytes 2097152

commit v2 on v1

v2 whole, which is shorter than its diff:
```python
import functools

import jax
import jax.numpy as jnp
from jax import lax
from jax.experimental import pallas as pl
from jax.experimental.pallas import tpu as pltpu
from jax.sharding import PartitionSpec as P

NORM_EPSILON = 1e-06
MESH = pl.DeviceIdType.MESH
CORES = 2
LANES = 128
VMEM = pltpu.VMEM


def greet(devices):
    barrier = pltpu.get_barrier_semaphore()
    for sp, tp in devices:
        pl.semaphore_signal(barrier, inc=1, device_id=(sp, tp), device_id_type=MESH)
    pl.semaphore_wait(barrier, len(devices))


def mesh_copy(src, dst, send, recv, device):
    return pltpu.make_async_remote_copy(
        src, dst, send, recv, device_id=device, device_id_type=MESH
    )


def layer_kernel(
    plan, tokens_ref, mix_ref, query_gain_ref, key_gain_ref, taps_ref, conv_gain_ref, gates_ref,
    attn_gain_ref, *refs
):
    sp_count, tp_count, head_count, head_dim, piece, sub = plan
    weight_refs = refs[:8]
    out_ref = refs[8]
    (
        weights, attn_weight, conv_weight, gathered, scaled, row_scales, kv_send, query_send,
        side_send, outer, padded, edge_send, edge_recv, kv_in, query_in, side_in, conv_mixed,
        done, landed, rhs, gates, scores_a, scores_b, flipped, attn, partial, keep, mate_out,
        mate_in, link_out, link_in,
        weight_sem, own_sem, cross_send, mate_send, tok_pass_send, tok_recv,
        kv_ssem, kv_rsem, query_ssem, query_rsem, side_ssem, side_rsem,
        kv_psem, kv_prsem, side_psem, side_prsem, local, edge_sem,
        send, recv, stay_sem, mate_ssem, mate_rsem, link_ssem, link_rsem,
    ) = refs[9:]
    f32 = jnp.float32
    bf16 = jnp.bfloat16
    sp = lax.axis_index("sp")
    tp = lax.axis_index("tp")
    core = lax.rem(tp, CORES)
    mate = tp + 1 - 2 * core
    first = tp - core
    chips = tp_count // CORES
    targets = sp_count // CORES
    rows, features = tokens_ref.shape
    width = head_count * head_dim
    half = LANES
    chunk = 2 * half
    chunks = rows // chunk
    pieces = rows // piece
    share = pieces // CORES
    phases = min(2, piece // half)
    tile = piece // phases
    slabs = piece // half
    span = 256
    both_tiles = 2 * tile
    block_rows = rows // tp_count
    subs = block_rows // phases // sub
    order = [chunks - 1] + list(range(chunks - 1))
    home = sp // targets
    slot = lax.rem(sp, targets) * CORES + core
    owner = home == core
    place_here = lax.rem(sp, share) * CORES + core
    query_gain = jnp.concatenate([query_gain_ref[...]] * head_count, axis=1)
    key_gain = jnp.concatenate([key_gain_ref[...]] * head_count, axis=1)

    mine = pltpu.make_async_copy(tokens_ref, gathered.at[tp], own_sem)
    mine.start()
    loads = [
        pltpu.make_async_copy(
            ref, (list(weights.at[i] for i in range(6)) + [attn_weight, conv_weight])[index],
            weight_sem.at[index],
        )
        for index, ref in enumerate(weight_refs)
    ]
    for index in (1, 2, 0, 3, 4, 5, 6, 7):
        loads[index].start()
    padded[0:8, :] = jnp.zeros((8, width), f32)
    for head in range(head_count):
        lines = [
            gates_ref[head : head + 1, row * LANES : (row + 1) * LANES]
            for row in range(rows // LANES)
        ]
        gain_line = attn_gain_ref[:, head * head_dim : (head + 1) * head_dim]
        gain_line = jnp.concatenate([gain_line, jnp.zeros((1, LANES - head_dim), f32)], axis=1)
        lines.append(jnp.broadcast_to(gain_line, (8, LANES)))
        side_send[head, :, :] = jnp.concatenate(lines, axis=0)
    greet(
        [
            (lax.rem(sp + step, sp_count), first + lax.rem(core + other, CORES))
            for step in range(sp_count)
            for other in range(CORES)
            if step or other
        ]
        + [(sp, lax.rem(tp + CORES * step, tp_count)) for step in range(1, chips)]
    )

    def block(number):
        return pl.ds(number * chunk, chunk)

    def tokens_to(device, number, sem):
        return mesh_copy(
            gathered.at[tp, block(number)], gathered.at[tp, block(number)], sem,
            tok_recv.at[tp, number], device,
        )

    def to_mate_tokens(number):
        return tokens_to((sp, mate), number, mate_send.at[number])

    def across_tokens(step, number):
        return tokens_to(
            (sp, lax.rem(tp + CORES * step, tp_count)), number, cross_send.at[step - 1, number]
        )

    def token_pass(step, number):
        other = lax.rem(tp + CORES * step, tp_count)
        return mesh_copy(
            gathered.at[other, block(number)], gathered.at[other, block(number)],
            tok_pass_send.at[step - 1, number], tok_recv.at[other, number], (sp, mate),
        )

    def token_arrival(source, number):
        return mesh_copy(
            gathered.at[source, block(number)], gathered.at[source, block(number)],
            mate_send.at[number], tok_recv.at[source, number], (sp, mate),
        )

    mine.wait()
    for number in order:
        for step in range(1, chips):
            across_tokens(step, number).start()
        to_mate_tokens(number).start()

    def target_of(step):
        at = lax.rem(sp + 1 + step, targets)
        return at // share, core * targets + at

    def side_copy(step, head, target):
        return mesh_copy(
            side_send.at[head], side_in.at[sp], side_ssem.at[step], side_rsem.at[sp], (target, tp)
        )

    def kv_copy(step, number, head, target):
        return mesh_copy(
            kv_send.at[head, block(number)], kv_in.at[sp, block(number)],
            kv_ssem.at[step, number], kv_rsem.at[sp, number], (target, tp),
        )

    def kept(number, head):
        return pltpu.make_async_copy(
            kv_send.at[head, block(number)], kv_in.at[sp, block(number)], local.at[number]
        )

    def kept_side(head):
        return pltpu.make_async_copy(side_send.at[head], side_in.at[sp], local.at[chunks])

    def slab_copies(slab, starting):
        spot, inner = slab // slabs, slab % slabs
        place = jnp.where(lax.rem(sp, 2) == 0, spot, pieces - 1 - spot)
        part = pl.ds(slab * head_dim, head_dim)
        for step in range(head_count):
            head = lax.rem(sp + 1 + step, head_count)
            target = core * targets + head * share + place // CORES
            there = first + lax.rem(place, CORES)
            here = jnp.logical_and(target == sp, there == tp)

            if starting:

                @pl.when(here)
                def _():
                    pltpu.make_async_copy(
                        query_send.at[head, part], query_in.at[sp, inner],
                        query_rsem.at[sp, inner],
                    ).start()

            @pl.when(jnp.logical_not(here))
            def _():
                copy = mesh_copy(
                    query_send.at[head, part], query_in.at[sp, inner],
                    query_ssem.at[step, slab], query_rsem.at[sp, inner], (target, there),
                )
                if starting:
                    copy.start()
                else:
                    copy.wait_send()

    def query_arrival(source, inner):
        mesh_copy(
            query_send.at[0, pl.ds(0, head_dim)], query_in.at[source, inner],
            query_ssem.at[0, 0], query_rsem.at[source, inner], (sp, mate),
        ).wait_recv()

    for step in range(targets):
        head, target = target_of(step)

        @pl.when(target != sp)
        def _():
            side_copy(step, head, target).start()

        @pl.when(target == sp)
        def _():
            kept_side(head).start()

    ones_row = lax.broadcasted_iota(jnp.int32, (width, width), 0) // head_dim
    ones_column = lax.broadcasted_iota(jnp.int32, (width, width), 1) // head_dim
    spread_mean = jnp.where(ones_row == ones_column, 1.0 / head_dim, 0.0).astype(bf16)

    def normed(values, gain):
        squares = values * values
        high = squares.astype(bf16)
        low = (squares - high.astype(f32)).astype(bf16)
        mean = jnp.dot(high, spread_mean, preferred_element_type=f32)
        mean = mean + jnp.dot(low, spread_mean, preferred_element_type=f32)
        return values * lax.rsqrt(mean + NORM_EPSILON) * gain

    def project(number, index):
        product = jnp.dot(
            scaled[block(number), :], weights[index], preferred_element_type=f32
        )
        return product * row_scales[block(number), 0:1]

    def take_tokens(number):
        here = block(number)
        for step in range(1, chips):
            token_arrival(lax.rem(tp + CORES * step, tp_count), number).wait_recv()
            token_pass(step, number).start()
        token_arrival(mate, number).wait_recv()
        for step in range(1, chips):
            token_arrival(lax.rem(mate + CORES * step, tp_count), number).wait_recv()
        total = jnp.zeros((chunk, 1), f32)
        for source in range(tp_count):
            part = gathered[source, here, :].astype(f32)
            at = slice(source * features, (source + 1) * features)
            total = total + jnp.sum(part * part, axis=1, keepdims=True)
            scaled[here, at] = (part * mix_ref[:, at]).astype(bf16)
        row_scale = lax.rsqrt(total / (tp_count * features) + NORM_EPSILON)
        row_scales[here, :] = jnp.broadcast_to(row_scale, (chunk, LANES))

    def send_keys(number):
        keys = normed(project(number, 1), key_gain).astype(bf16)
        values = project(number, 2)
        for head in range(head_count):
            at = slice(head * head_dim, (head + 1) * head_dim)
            kv_send[head, pl.ds(number * chunk, half), :] = jnp.concatenate(
                [keys[:half, at], keys[half:, at]], axis=1
            )
        for side in range(2):
            rows_of = slice(side * half, (side + 1) * half)
            for lane in range(0, width, LANES):
                turned = values[rows_of, lane : lane + LANES].T.astype(bf16)
                for inner in range(LANES // head_dim):
                    kv_send[
                        lane // head_dim + inner,
                        pl.ds(number * chunk + half + side * head_dim, head_dim),
                        :,
                    ] = turned[inner * head_dim : (inner + 1) * head_dim]
        for step in range(targets):
            head, target = target_of(step)

            @pl.when(target != sp)
            def _():
                kv_copy(step, number, head, target).start()

            @pl.when(target == sp)
            def _():
                kept(number, head).start()

    def send_queries(number):
        queries = normed(project(number, 0), query_gain).astype(bf16)
        queries = queries.astype(f32) * head_dim ** (-0.5)
        for side in range(2):
            rows_of = slice(side * half, (side + 1) * half)
            for lane in range(0, width, LANES):
                turned = queries[rows_of, lane : lane + LANES].T.astype(bf16)
                for inner in range(LANES // head_dim):
                    query_send[
                        lane // head_dim + inner,
                        pl.ds(number * half + side * head_dim, head_dim),
                        :,
                    ] = turned[inner * head_dim : (inner + 1) * head_dim]
        slab_copies(2 * number, True)

    for index in (1, 2, 0):
        loads[index].wait()
    for number in order:
        take_tokens(number)
        send_keys(number)
        send_queries(number)
    for number in order:
        slab_copies(2 * number + 1, True)

    sources = [lax.rem(sp + step, sp_count) for step in range(sp_count)]

    def kv_pass(source, number):
        return mesh_copy(
            kv_in.at[source, block(number)], kv_in.at[source, block(number)],
            kv_psem.at[source, number], kv_prsem.at[source, number], (sp, mate),
        )

    def side_pass(source):
        return mesh_copy(
            side_in.at[source], side_in.at[source], side_psem.at[source], side_prsem.at[source],
            (sp, mate),
        )

    @pl.when(owner)
    def _():
        for step, source in enumerate(sources):
            if step == 0:
                kept_side(0).wait()
            else:
                mesh_copy(
                    side_send.at[0], side_in.at[source], side_ssem.at[0], side_rsem.at[source],
                    (sp, mate),
                ).wait_recv()
            side_pass(source).start()

    @pl.when(jnp.logical_not(owner))
    def _():
        for source in sources:
            side_pass(source).wait_recv()

    def forward(number):
        @pl.when(owner)
        def _():
            for step, source in enumerate(sources):
                if step == 0:
                    kept(number, 0).wait()
                else:
                    mesh_copy(
                        kv_send.at[0, block(number)], kv_in.at[source, block(number)],
                        kv_ssem.at[0, number], kv_rsem.at[source, number], (sp, mate),
                    ).wait_recv()
                kv_pass(source, number).start()

    gain_tile = jnp.broadcast_to(side_in[0, rows // LANES : rows // LANES + 1, :], (LANES, LANES))
    gain = gain_tile.T[:head_dim, 0:1]

    def pieces_of(values):
        high = values.astype(bf16).astype(f32)
        middle = (values - high).astype(bf16).astype(f32)
        low = (values - high - middle).astype(bf16).astype(f32)
        return high, middle, low

    def gate_columns(source, _):
        cuts = pieces_of(-side_in[source, : rows // LANES, :])
        for number in range(chunks):
            lines = [
                cut[2 * number + side : 2 * number + side + 1, :] for side in range(2) for cut in cuts
            ]
            lines.append(jnp.zeros((LANES - len(lines), LANES), f32))
            gates[source, number * half : (number + 1) * half, :] = (
                jnp.concatenate(lines, axis=0).T.astype(bf16)
            )
        return 0

    forward(order[0])
    lax.fori_loop(0, sp_count, gate_columns, 0)

    def conv_inputs(number):
        here = block(number)
        outer[here, :] = project(number, 3)
        gated = (project(number, 4) * project(number, 5)).astype(bf16)
        padded[pl.ds(8 + number * chunk, chunk), :] = gated.astype(f32)
        return gated

    edge = mesh_copy(
        edge_send, edge_recv, edge_sem.at[0], edge_sem.at[1], (lax.rem(sp + 1, sp_count), tp)
    )
    for index in (3, 4, 5):
        loads[index].wait()
    for position, number in enumerate(order):
        gated = conv_inputs(number)
        if position == 0:
            edge_send[...] = gated[chunk - 16 :, :]

            @pl.when(sp < sp_count - 1)
            def _():
                edge.start()

        elif position < chunks - 1:
            forward(number)

    @pl.when(sp > 0)
    def _():
        edge.wait_recv()
        padded[0:8, :] = edge_recv[8:16, :].astype(f32)

    taps = taps_ref.shape[0]
    for number in range(chunks):
        convolved = jnp.zeros((chunk, width), f32)
        for tap in range(taps):
            at = pl.ds(8 - taps + 1 + tap + number * chunk, chunk)
            convolved = convolved + taps_ref[tap : tap + 1, :] * padded[at, :]
        conv_mixed[block(number), :] = normed(
            outer[block(number), :] * convolved, conv_gain_ref[...]
        ).astype(bf16)
    loads[6].wait()
    loads[7].wait()
    for number in range(tp_count):
        at = pl.ds(number * block_rows, block_rows)
        partial[at, :] = jnp.dot(conv_mixed[at, :], conv_weight[...], preferred_element_type=f32)
    forward(order[-1])

    @pl.when(jnp.logical_not(owner))
    def _():
        for source in sources:
            for number in order:
                kv_pass(source, number).wait_recv()

    def away(phase, source):
        return mesh_copy(
            done.at[phase, source], landed.at[phase, slot], send.at[phase, source],
            recv.at[phase, slot], (source, first + home),
        )

    def stay(phase, source, index):
        return pltpu.make_async_copy(
            done.at[phase, source], landed.at[phase, index], stay_sem.at[phase]
        )

    def queries_of(phase, source):
        return jnp.concatenate(
            [query_in[source, slab, :, :] for slab in range(phase, slabs, phases)], axis=1
        )

    def set_queries(phase, even, odd):
        queries = jnp.concatenate([queries_of(phase, even), queries_of(phase, odd)], axis=1)
        empty = jnp.zeros_like(queries)
        row = lax.broadcasted_iota(jnp.int32, (LANES, both_tiles), 0)
        for side in range(2):
            ones = jnp.logical_and(row >= 3 * side, row < 3 * side + 3)
            stacked = [queries, empty] if side == 0 else [empty, queries]
            rhs[side, :, :] = jnp.concatenate(
                stacked + [jnp.where(ones, 1.0, 0.0).astype(bf16)], axis=0
            )

    def score(source, side, scores, top, limit):
        key_rows = jnp.concatenate(
            [kv_in[source, pl.ds(number * chunk, half), :] for number in range(rows // chunk)],
            axis=0,
        )
        lhs = jnp.concatenate([key_rows, gates[source, :, :]], axis=1)
        part = jnp.dot(lhs, rhs[side, :, :], preferred_element_type=f32)
        if limit is not None:
            row = lax.broadcasted_iota(jnp.int32, part.shape, 0)
            row = row // half * chunk + lax.rem(row, half) + side * half
            part = jnp.where(row <= limit, part, -jnp.inf)
        scores[side * (rows // 2) : (side + 1) * (rows // 2), :] = part
        return jnp.maximum(top, jnp.max(part.reshape(-1, 8, both_tiles), axis=0))

    def blend(source, scores, side, begin, top, total):
        start = side * (rows // 2) + begin * half
        weights = jnp.exp(scores[start : start + span, :] - top).astype(bf16)
        values = jnp.concatenate(
            [
                kv_in[source, pl.ds((begin + index) * chunk + half + side * head_dim, head_dim), :]
                for index in range(span // half)
            ],
            axis=1,
        )
        return total + jnp.dot(values, weights, preferred_element_type=f32)

    def start_top():
        return jnp.full((8, both_tiles), -jnp.inf, f32)

    def settle_top(top):
        return jnp.max(top, axis=0, keepdims=True)

    def advance(old, old_scores, old_top, state, new, new_scores, limit=None):
        top = jnp.maximum(state[0], old_top)
        total = state[1] * jnp.exp(state[0] - top)
        new_top = start_top()
        for side in range(2):
            if new is not None:
                new_top = score(new, side, new_scores, new_top, limit)
            for begin in range(0, rows // chunk, span // half):
                total = blend(old, old_scores, side, begin, top, total)
        return (top, total), settle_top(new_top)

    def finish(phase, source, attended):
        scale = lax.rsqrt(jnp.mean(attended * attended, axis=0, keepdims=True) + NORM_EPSILON)
        done[phase, source, :, :] = (attended * scale * gain).astype(bf16)
        stays = jnp.logical_and(source == sp, owner)

        @pl.when(stays)
        def _():
            stay(phase, source, slot).start()

        @pl.when(jnp.logical_not(stays))
        def _():
            away(phase, source).start()

    def attend(phase):
        for source in range(sp_count):
            for inner in range(phase, slabs, phases):
                query_arrival(source, inner)
        column = lax.broadcasted_iota(jnp.int32, (1, both_tiles), 1)
        inside = lax.rem(column, tile)
        inside = (inside // half * phases + phase) * half + lax.rem(inside, half)
        in_even = column < tile
        even_limit = jnp.where(in_even, inside + place_here * piece, rows)
        odd_limit = jnp.where(in_even, -1, inside + (pieces - 1 - place_here) * piece)
        empty = (
            jnp.full((1, both_tiles), -1e30, f32), jnp.zeros((head_dim, both_tiles), f32)
        )

        def pair_of_sources(pair, carried):
            state, top, last = carried
            even, odd = 2 * pair, 2 * pair + 1
            set_queries(phase, even, odd)
            state, top = advance(last, scores_b, top, state, even, scores_a, even_limit)

            @pl.when(pair > 0)
            def _():
                finish(phase, even - 2, state[1][:, :tile])
                finish(phase, odd - 2, state[1][:, tile:])

            state, top = advance(even, scores_a, top, empty, odd, scores_b, odd_limit)

            def two_sources(step, carried):
                state, top, last = carried
                state, top = advance(last, scores_b, top, state, 2 * step, scores_a)
                state, top = advance(2 * step, scores_a, top, state, 2 * step + 1, scores_b)
                return state, top, 2 * step + 1

            return lax.fori_loop(0, pair, two_sources, (state, top, odd))

        if phase == 0:
            scores_b[...] = jnp.zeros_like(scores_b)
        state, top, last = lax.fori_loop(
            0, sp_count // 2, pair_of_sources, (empty, jnp.zeros((1, both_tiles), f32), 0)
        )
        state, _ = advance(last, scores_b, top, state, None, None)
        finish(phase, sp_count - 2, state[1][:, :tile])
        finish(phase, sp_count - 1, state[1][:, tile:])

    def arrive(phase):
        for index in range(targets * CORES):
            giver = core * targets + index // CORES
            here = jnp.logical_and(giver == sp, core == index % CORES)

            @pl.when(here)
            def _():
                stay(phase, 0, index).wait()

            @pl.when(jnp.logical_not(here))
            def _():
                mesh_copy(
                    done.at[phase, 0], landed.at[phase, index], send.at[phase, 0],
                    recv.at[phase, index], (sp, mate),
                ).wait_recv()

            head = index // (share * CORES)
            place = index % (share * CORES)
            spot = jnp.where(lax.rem(sp, 2) == 0, place, pieces - 1 - place)
            for inner in range(tile // half):
                start = pl.multiple_of((spot * slabs + inner * phases + phase) * half, half)
                flipped[head * head_dim : (head + 1) * head_dim, pl.ds(start, half)] = landed[
                    phase, index, :, inner * half : (inner + 1) * half
                ]
        for slab in range(phase, rows // half, phases):
            at = slice(slab * half, (slab + 1) * half)
            attn[at, :] = flipped[:, at].astype(f32).T.astype(bf16)

    def product(block, number):
        at = pl.ds(pl.multiple_of(block * block_rows + number * sub, sub), sub)
        return partial[at, :] + jnp.dot(
            attn[at, :], attn_weight[...], preferred_element_type=f32
        )

    def within(number):
        return pl.ds(number * sub, sub)

    def to_mate(step, number):
        at = within(number)
        return mesh_copy(
            mate_out.at[step, at], mate_in.at[step, at], mate_ssem.at[step, number],
            mate_rsem.at[step, number], (sp, mate),
        )

    def across(step, number):
        at = within(number)
        return mesh_copy(
            link_out.at[step - 1, at], link_in.at[step - 1, at], link_ssem.at[step - 1, number],
            link_rsem.at[step - 1, number], (sp, lax.rem(tp + CORES * step, tp_count)),
        )

    def joined(step, number):
        at = within(number)
        to_mate(step, number).wait_recv()
        total = keep[step, at, :] + mate_in[step, at, :].astype(f32)
        link_out[step - 1, at, :] = total.astype(bf16)
        across(step, number).start()

    def spread(phase):
        waiting = []
        for step in list(range(1, chips)) + [0]:
            for number in range(phase * subs, (phase + 1) * subs):
                at = within(number)
                theirs = lax.rem(mate + CORES * step, tp_count)
                ours = lax.rem(tp + CORES * step, tp_count)
                mate_out[step, at, :] = product(theirs, number).astype(bf16)
                to_mate(step, number).start()
                keep[step, at, :] = product(ours, number)
                if waiting:
                    joined(*waiting.pop())
                if step:
                    waiting.append((step, number))

    def settle(phase):
        for number in range(phase * subs, (phase + 1) * subs):
            at = within(number)
            to_mate(0, number).wait_recv()
            total = keep[0, at, :] + mate_in[0, at, :].astype(f32)
            for step in range(1, chips):
                across(step, number).wait_recv()
                total = total + link_in[step - 1, at, :].astype(f32)
            out_ref[at, :] = total.astype(bf16)

    attend(0)
    arrive(0)
    spread(0)
    for phase in range(1, phases):
        attend(phase)
        settle(phase - 1)
        arrive(phase)
        spread(phase)
    settle(phases - 1)
    for step in range(chips):
        for number in range(phases * subs):
            to_mate(step, number).wait_send()
            if step:
                across(step, number).wait_send()
    for phase in range(phases):
        for step in range(1, sp_count):
            away(phase, lax.rem(sp + step, sp_count)).wait_send()

        @pl.when(jnp.logical_not(owner))
        def _():
            away(phase, sp).wait_send()

    @pl.when(owner)
    def _():
        for source in sources:
            side_pass(source).wait_send()
            for number in order:
                kv_pass(source, number).wait_send()

    for step in range(targets):
        head, target = target_of(step)

        @pl.when(target != sp)
        def _():
            side_copy(step, head, target).wait_send()
            for number in order:
                kv_copy(step, number, head, target).wait_send()

    for slab in range(2 * chunks):
        slab_copies(slab, False)
    for number in order:
        to_mate_tokens(number).wait_send()
        for step in range(1, chips):
            across_tokens(step, number).wait_send()
            token_pass(step, number).wait_send()

    @pl.when(sp < sp_count - 1)
    def _():
        edge.wait_send()


def layer(
    tokens, mix_gain, query_gain, key_gain, taps, conv_gain, gate_rows, attn_gain, weights, head_dim
):
    sp_count = lax.axis_size("sp")
    tp_count = lax.axis_size("tp")
    rows, features = tokens.shape
    width = weights[0].shape[1]
    out_features = weights[6].shape[1]
    heads = width // head_dim
    pieces = sp_count // heads
    piece = rows // pieces
    phases = min(2, piece // LANES)
    tile = piece // phases
    slabs = piece // LANES
    chunks = rows // LANES // 2
    chips = tp_count // CORES
    targets = sp_count // CORES
    block_rows = rows // tp_count
    sub = min(64, block_rows // 2)
    subs = block_rows // sub
    links = max(chips - 1, 1)
    bf16 = jnp.bfloat16
    f32 = jnp.float32
    dma = pltpu.SemaphoreType.DMA
    vmem = pl.BlockSpec(memory_space=VMEM)
    hbm = pl.BlockSpec(memory_space=pl.ANY)
    return pl.pallas_call(
        functools.partial(layer_kernel, (sp_count, tp_count, heads, head_dim, piece, sub)),
        out_shape=jax.ShapeDtypeStruct((block_rows, out_features), bf16),
        in_specs=[hbm] + [vmem] * 7 + [hbm] * 8,
        out_specs=vmem,
        scratch_shapes=[
            VMEM((6,) + weights[0].shape, bf16),
            VMEM(weights[6].shape, bf16),
            VMEM(weights[7].shape, bf16),
            VMEM((tp_count, rows, features), bf16),
            VMEM((rows, tp_count * features), bf16),
            VMEM((rows, LANES), f32),
            VMEM((heads, rows, LANES), bf16),
            VMEM((heads, rows // 2, LANES), bf16),
            VMEM((heads, rows // LANES + 8, LANES), f32),
            VMEM((rows, width), f32),
            VMEM((rows + 8, width), f32),
            VMEM((16, width), bf16),
            VMEM((16, width), bf16),
            VMEM((sp_count, rows, LANES), bf16),
            VMEM((sp_count, slabs, head_dim, LANES), bf16),
            VMEM((sp_count, rows // LANES + 8, LANES), f32),
            VMEM((rows, width), bf16),
            VMEM((phases, sp_count, head_dim, tile), bf16),
            VMEM((phases, sp_count, head_dim, tile), bf16),
            VMEM((2, 2 * LANES, 2 * tile), bf16),
            VMEM((sp_count, rows // 2, LANES), bf16),
            VMEM((rows, 2 * tile), f32),
            VMEM((rows, 2 * tile), f32),
            VMEM((width, rows), bf16),
            VMEM((rows, width), bf16),
            VMEM((rows, out_features), f32),
            VMEM((chips, block_rows, out_features), f32),
            VMEM((chips, block_rows, out_features), bf16),
            VMEM((chips, block_rows, out_features), bf16),
            VMEM((links, block_rows, out_features), bf16),
            VMEM((links, block_rows, out_features), bf16),
            dma((8,)), dma, dma((links, chunks)), dma((chunks,)), dma((links, chunks)),
            dma((tp_count, chunks)),
            dma((targets, chunks)), dma((sp_count, chunks)),
            dma((heads, 2 * chunks)), dma((sp_count, slabs)),
            dma((targets,)), dma((sp_count,)),
            dma((sp_count, chunks)), dma((sp_count, chunks)),
            dma((sp_count,)), dma((sp_count,)),
            dma((chunks + 1,)), dma((2,)),
            dma((phases, sp_count)), dma((phases, sp_count)), dma((phases,)),
            dma((chips, subs)), dma((chips, subs)), dma((links, subs)), dma((links, subs)),
        ],
        compiler_params=pltpu.CompilerParams(
            collective_id=0, has_side_effects=True, vmem_limit_bytes=63 * 1024 * 1024
        ),
    )(tokens, mix_gain, query_gain, key_gain, taps, conv_gain, gate_rows, attn_gain, *weights)


def per_device(
    tokens,
    mix_gain,
    query_weight,
    key_weight,
    value_weight,
    outer_gate_weight,
    inner_gate_weight,
    conv_input_weight,
    query_gain,
    key_gain,
    gate_totals,
    conv_taps,
    attn_out_gain,
    conv_out_gain,
    attn_out_weight,
    conv_out_weight,
):
    return layer(
        tokens,
        mix_gain.reshape(1, -1),
        query_gain.reshape(1, -1),
        key_gain.reshape(1, -1),
        conv_taps,
        conv_out_gain.reshape(1, -1),
        gate_totals.T,
        attn_out_gain.reshape(1, -1),
        (
            query_weight,
            key_weight,
            value_weight,
            outer_gate_weight,
            inner_gate_weight,
            conv_input_weight,
            attn_out_weight,
            conv_out_weight,
        ),
        query_gain.shape[0],
    )


def solution(mesh):
    placed = (
        P("sp", "tp"),
        P(),
        P(None, "tp"),
        P(None, "tp"),
        P(None, "tp"),
        P(None, "tp"),
        P(None, "tp"),
        P(None, "tp"),
        P(),
        P(),
        P("sp", "tp"),
        P(None, "tp"),
        P("tp"),
        P("tp"),
        P("tp", None),
        P("tp", None),
    )
    return jax.shard_map(
        per_device, mesh=mesh, in_specs=placed, out_specs=P(("sp", "tp"), None), check_vma=False
    )
```

time: 122 us -> 112 us (0.918)
  the two profiles are of different devices: /device:TPU:26 before, /device:TPU:24 now
where the time goes in v2:
time: 112 us; the launch traced here: 111 us
  Pallas kernels  109 us (97%)
  local copies, waits for them, and re-layouts  2.3 us (2%)
    pallas_call x1, Pallas kernels, layer(): pl.pallas_call(functools.partial(layer_kernel, (sp_count, tp_count, heads...  109 us
    unnamed x1, local copies, waits for them, and re-layouts  2.3 us

profile of v2, /device:TPU:24, one launch (start us, length us, event | category | flops | bytes accessed | tf_op | source)
XLA Modules:
  0.0 111.3 jit_solution(18107542699690669369)
XLA Ops:
  0.0 109.0 %shard_map.154 = bf16[256,2048]{1,0:T(8,128)(2,1)} custom-call(bf16[1024,512]{1,0:T(8,128)(2,1)} %tokens_ref.1, f32[1,2048]{1,0:T(1,128)} %bitcast.7, f32[1,64]{1,0:T(1,128)} %bitcast.10, f32[1,64]{1,0:T(1,128)} %bitcast.11, f32[3,256]{1,0:T(4,128)} %taps_ref.1, f32[1,256]{1,0:T(1,128)} %bitcast.8, f32[4,1024]{1,0:T(4,128)} %bitcast.6, f32[1,256]{1,0:T(1,128)} %bitcast.9, ...), custom_call_target="tpu_custom_call" | custom-call | tf_op jit(solution)/shard_map/pallas_call | solution.py:709
  109.0 2.3 %copy.18 = bf16[256,2048]{1,0:T(8,128)(2,1)} copy(bf16[256,2048]{1,0:T(8,128)(2,1)} %shard_map.154) | data formatting | bytes 2097152

commit v3 on v2

--- a/solution.py
+++ b/solution.py
@@ -31,18 +31,17 @@
     plan, tokens_ref, mix_ref, query_gain_ref, key_gain_ref, taps_ref, conv_gain_ref, gates_ref,
     attn_gain_ref, *refs
 ):
-    sp_count, tp_count, head_count, head_dim, piece, sub = plan
+    sp_count, tp_count, head_count, head_dim, piece = plan
     weight_refs = refs[:8]
     out_ref = refs[8]
     (
-        weights, attn_weight, conv_weight, gathered, scaled, row_scales, kv_send, query_send,
+        weights, out_weights, gathered, scaled, row_scales, kv_send, query_send,
         side_send, outer, padded, edge_send, edge_recv, kv_in, query_in, side_in, conv_mixed,
-        done, landed, rhs, gates, scores_a, scores_b, flipped, attn, partial, keep, mate_out,
-        mate_in, link_out, link_in,
+        conv_in, done, landed, rhs, gates, scores_a, scores_b, conv_rows,
         weight_sem, own_sem, cross_send, mate_send, tok_pass_send, tok_recv,
         kv_ssem, kv_rsem, query_ssem, query_rsem, side_ssem, side_rsem,
         kv_psem, kv_prsem, side_psem, side_prsem, local, edge_sem,
-        send, recv, stay_sem, mate_ssem, mate_rsem, link_ssem, link_rsem,
+        send, recv, conv_ssem, conv_rsem, out_recv, out_cross, out_side, out_mate,
     ) = refs[9:]
     f32 = jnp.float32
     bf16 = jnp.bfloat16
@@ -66,10 +65,13 @@
     span = 256
     both_tiles = 2 * tile
     block_rows = rows // tp_count
-    subs = block_rows // phases // sub
+    parts = 4
+    part_rows = width // parts
+    parity = lax.rem(sp, 2)
+    beside = sp + 1 - 2 * parity
     order = [chunks - 1] + list(range(chunks - 1))
     home = sp // targets
-    slot = lax.rem(sp, targets) * CORES + core
+    head_slot = (first + home) * head_count + lax.rem(sp, targets) // share
     owner = home == core
     place_here = lax.rem(sp, share) * CORES + core
     query_gain = jnp.concatenate([query_gain_ref[...]] * head_count, axis=1)
@@ -79,7 +81,10 @@
     mine.start()
     loads = [
         pltpu.make_async_copy(
-            ref, (list(weights.at[i] for i in range(6)) + [attn_weight, conv_weight])[index],
+            ref,
+            weights.at[index]
+            if index < 6
+            else out_weights.at[index - 6, pl.ds(pl.multiple_of(tp * width, width), width)],
             weight_sem.at[index],
         )
         for index, ref in enumerate(weight_refs)
@@ -98,12 +103,11 @@
         side_send[head, :, :] = jnp.concatenate(lines, axis=0)
     greet(
         [
-            (lax.rem(sp + step, sp_count), first + lax.rem(core + other, CORES))
+            (lax.rem(sp + step, sp_count), lax.rem(tp + other, tp_count))
             for step in range(sp_count)
-            for other in range(CORES)
+            for other in range(tp_count)
             if step or other
         ]
-        + [(sp, lax.rem(tp + CORES * step, tp_count)) for step in range(1, chips)]
     )
 
     def block(number):
@@ -300,6 +304,48 @@
     for number in order:
         slab_copies(2 * number + 1, True)
 
+    def part_of(kind, source, part):
+        at = pl.multiple_of(source * width + part * part_rows, part_rows)
+        return out_weights.at[kind, pl.ds(at, part_rows)]
+
+    def weights_to(kind, source, part, sem, device):
+        ref = part_of(kind, source, part)
+        return mesh_copy(ref, ref, sem, out_recv.at[kind, source, part], device)
+
+    def weights_across(step, part):
+        return weights_to(
+            parity, tp, part, out_cross.at[step - 1, part],
+            (sp, lax.rem(tp + CORES * step, tp_count)),
+        )
+
+    def weights_beside(step, part):
+        source = lax.rem(tp + CORES * step, tp_count)
+        return weights_to(parity, source, part, out_side.at[step - 1, part], (beside, tp))
+
+    def weights_mate(kind, source, part):
+        return weights_to(kind, source, part, out_mate.at[kind, source, part], (sp, mate))
+
+    def from_across(part):
+        for step in range(1, chips):
+            source = lax.rem(tp + CORES * step, tp_count)
+            weights_mate(parity, source, part).wait_recv()
+            weights_beside(step, part).start()
+            weights_mate(parity, source, part).start()
+
+    def from_beside(part):
+        for step in range(1, chips):
+            source = lax.rem(tp + CORES * step, tp_count)
+            weights_mate(1 - parity, source, part).wait_recv()
+            weights_mate(1 - parity, source, part).start()
+
+    loads[6].wait()
+    loads[7].wait()
+    for step in range(1, chips):
+        for number in order:
+            across_tokens(step, number).wait_send()
+        for part in range(parts):
+            weights_across(step, part).start()
+
     sources = [lax.rem(sp + step, sp_count) for step in range(sp_count)]
 
     def kv_pass(source, number):
@@ -406,11 +452,19 @@
         conv_mixed[block(number), :] = normed(
             outer[block(number), :] * convolved, conv_gain_ref[...]
         ).astype(bf16)
-    loads[6].wait()
-    loads[7].wait()
-    for number in range(tp_count):
-        at = pl.ds(number * block_rows, block_rows)
-        partial[at, :] = jnp.dot(conv_mixed[at, :], conv_weight[...], preferred_element_type=f32)
+
+    def conv_share(step):
+        there = lax.rem(tp + step, tp_count)
+        at = pl.ds(pl.multiple_of(there * block_rows, block_rows), block_rows)
+        return mesh_copy(
+            conv_mixed.at[at], conv_in.at[tp], conv_ssem.at[step - 1], conv_rsem.at[tp],
+            (sp, there),
+        )
+
+    for step in range(1, tp_count):
+        conv_share(step).start()
+    own_rows = pl.ds(pl.multiple_of(tp * block_rows, block_rows), block_rows)
+    conv_in[tp, :, :] = conv_mixed[own_rows, :]
     forward(order[-1])
 
     @pl.when(jnp.logical_not(owner))
@@ -419,16 +473,28 @@
             for number in order:
                 kv_pass(source, number).wait_recv()
 
-    def away(phase, source):
+    for kind in range(2):
+        for part in range(parts):
+            weights_mate(kind, tp, part).start()
+    for part in range(parts // 2):
+        from_across(part)
+
+    def place_of(phase, inner, spot):
+        begin = (inner * phases + phase) * half
+        return spot * (piece // block_rows) + begin // block_rows, begin % block_rows
+
+    def away(phase, source, inner, spot):
+        there, at = place_of(phase, inner, spot)
         return mesh_copy(
-            done.at[phase, source], landed.at[phase, slot], send.at[phase, source],
-            recv.at[phase, slot], (source, first + home),
-        )
-
-    def stay(phase, source, index):
-        return pltpu.make_async_copy(
-            done.at[phase, source], landed.at[phase, index], stay_sem.at[phase]
-        )
+            done.at[phase, source, :, pl.ds(inner * half, half)],
+            landed.at[head_slot, :, pl.ds(at, half)],
+            send.at[phase, source, inner], recv.at[head_slot, at // half], (source, there),
+        )
+
+    def stays_here(phase, source, inner, spot):
+        return jnp.logical_and(source == sp, place_of(phase, inner, spot)[0] == tp)
+
+    even_spot, odd_spot = place_here, pieces - 1 - place_here
 
     def queries_of(phase, source):
         return jnp.concatenate(
@@ -489,18 +555,24 @@
                 total = blend(old, old_scores, side, begin, top, total)
         return (top, total), settle_top(new_top)
 
-    def finish(phase, source, attended):
+    def finish(phase, source, attended, spot):
         scale = lax.rsqrt(jnp.mean(attended * attended, axis=0, keepdims=True) + NORM_EPSILON)
         done[phase, source, :, :] = (attended * scale * gain).astype(bf16)
-        stays = jnp.logical_and(source == sp, owner)
-
-        @pl.when(stays)
-        def _():
-            stay(phase, source, slot).start()
-
-        @pl.when(jnp.logical_not(stays))
-        def _():
-            away(phase, source).start()
+        for inner in range(tile // half):
+            stays = stays_here(phase, source, inner, spot)
+
+            @pl.when(stays)
+            def _():
+                at = place_of(phase, inner, spot)[1]
+                pltpu.make_async_copy(
+                    done.at[phase, source, :, pl.ds(inner * half, half)],
+                    landed.at[head_slot, :, pl.ds(at, half)],
+                    recv.at[head_slot, at // half],
+                ).start()
+
+            @pl.when(jnp.logical_not(stays))
+            def _():
+                away(phase, source, inner, spot).start()
 
     def attend(phase):
         for source in range(sp_count):
@@ -510,8 +582,8 @@
         inside = lax.rem(column, tile)
         inside = (inside // half * phases + phase) * half + lax.rem(inside, half)
         in_even = column < tile
-        even_limit = jnp.where(in_even, inside + place_here * piece, rows)
-        odd_limit = jnp.where(in_even, -1, inside + (pieces - 1 - place_here) * piece)
+        even_limit = jnp.where(in_even, inside + even_spot * piece, rows)
+        odd_limit = jnp.where(in_even, -1, inside + odd_spot * piece)
         empty = (
             jnp.full((1, both_tiles), -1e30, f32), jnp.zeros((head_dim, both_tiles), f32)
         )
@@ -524,8 +596,8 @@
 
             @pl.when(pair > 0)
             def _():
-                finish(phase, even - 2, state[1][:, :tile])
-                finish(phase, odd - 2, state[1][:, tile:])
+                finish(phase, even - 2, state[1][:, :tile], even_spot)
+                finish(phase, odd - 2, state[1][:, tile:], odd_spot)
 
             state, top = advance(even, scores_a, top, empty, odd, scores_b, odd_limit)
 
@@ -543,113 +615,70 @@
             0, sp_count // 2, pair_of_sources, (empty, jnp.zeros((1, both_tiles), f32), 0)
         )
         state, _ = advance(last, scores_b, top, state, None, None)
-        finish(phase, sp_count - 2, state[1][:, :tile])
-        finish(phase, sp_count - 1, state[1][:, tile:])
-
-    def arrive(phase):
-        for index in range(targets * CORES):
-            giver = core * targets + index // CORES
-            here = jnp.logical_and(giver == sp, core == index % CORES)
-
-            @pl.when(here)
-            def _():
-                stay(phase, 0, index).wait()
-
-            @pl.when(jnp.logical_not(here))
-            def _():
+        finish(phase, sp_count - 2, state[1][:, :tile], even_spot)
+        finish(phase, sp_count - 1, state[1][:, tile:], odd_spot)
+
+    for phase in range(phases):
+        attend(phase)
+        if phase == 0:
+            for part in range(parts // 2, parts):
+                from_across(part)
+    for part in range(parts):
+        from_beside(part)
+    for step in range(1, tp_count):
+        source = lax.rem(tp + step, tp_count)
+        mesh_copy(
+            conv_mixed.at[pl.ds(0, block_rows)], conv_in.at[source], conv_ssem.at[0],
+            conv_rsem.at[source], (sp, mate),
+        ).wait_recv()
+    for step in range(chips):
+        source = lax.rem(mate + CORES * step, tp_count)
+        for kind in range(2):
+            for part in range(parts):
+                weights_mate(kind, source, part).wait_recv()
+    out_span = 512
+    out_features = out_ref.shape[1]
+    conv_rows_in = jnp.concatenate([conv_in[source, :, :] for source in range(tp_count)], axis=1)
+    for begin in range(0, out_features, out_span):
+        at = slice(begin, begin + out_span)
+        conv_rows[:, at] = jnp.dot(
+            conv_rows_in, out_weights[1, :, at], preferred_element_type=f32
+        )
+    for phase in range(phases):
+        for index in range(phase, block_rows // half, phases):
+            for source in range(tp_count * head_count):
                 mesh_copy(
-                    done.at[phase, 0], landed.at[phase, index], send.at[phase, 0],
-                    recv.at[phase, index], (sp, mate),
+                    done.at[0, 0, :, pl.ds(0, half)],
+                    landed.at[source, :, pl.ds(index * half, half)],
+                    send.at[0, 0, 0], recv.at[source, index], (sp, mate),
                 ).wait_recv()
-
-            head = index // (share * CORES)
-            place = index % (share * CORES)
-            spot = jnp.where(lax.rem(sp, 2) == 0, place, pieces - 1 - place)
+            here = slice(index * half, (index + 1) * half)
+            mixed = landed[:, :, here].reshape(tp_count * width, half)
+            mixed = mixed.astype(f32).T.astype(bf16)
+            for begin in range(0, out_features, out_span):
+                at = slice(begin, begin + out_span)
+                out_ref[here, at] = (
+                    conv_rows[here, at]
+                    + jnp.dot(mixed, out_weights[0, :, at], preferred_element_type=f32)
+                ).astype(bf16)
+    for phase in range(phases):
+        for source in range(sp_count):
             for inner in range(tile // half):
-                start = pl.multiple_of((spot * slabs + inner * phases + phase) * half, half)
-                flipped[head * head_dim : (head + 1) * head_dim, pl.ds(start, half)] = landed[
-                    phase, index, :, inner * half : (inner + 1) * half
-                ]
-        for slab in range(phase, rows // half, phases):
-            at = slice(slab * half, (slab + 1) * half)
-            attn[at, :] = flipped[:, at].astype(f32).T.astype(bf16)
-
-    def product(block, number):
-        at = pl.ds(pl.multiple_of(block * block_rows + number * sub, sub), sub)
-        return partial[at, :] + jnp.dot(
-            attn[at, :], attn_weight[...], preferred_element_type=f32
-        )
-
-    def within(number):
-        return pl.ds(number * sub, sub)
-
-    def to_mate(step, number):
-        at = within(number)
-        return mesh_copy(
-            mate_out.at[step, at], mate_in.at[step, at], mate_ssem.at[step, number],
-            mate_rsem.at[step, number], (sp, mate),
-        )
-
-    def across(step, number):
-        at = within(number)
-        return mesh_copy(
-            link_out.at[step - 1, at], link_in.at[step - 1, at], link_ssem.at[step - 1, number],
-            link_rsem.at[step - 1, number], (sp, lax.rem(tp + CORES * step, tp_count)),
-        )
-
-    def joined(step, number):
-        at = within(number)
-        to_mate(step, number).wait_recv()
-        total = keep[step, at, :] + mate_in[step, at, :].astype(f32)
-        link_out[step - 1, at, :] = total.astype(bf16)
-        across(step, number).start()
-
-    def spread(phase):
-        waiting = []
-        for step in list(range(1, chips)) + [0]:
-            for number in range(phase * subs, (phase + 1) * subs):
-                at = within(number)
-                theirs = lax.rem(mate + CORES * step, tp_count)
-                ours = lax.rem(tp + CORES * step, tp_count)
-                mate_out[step, at, :] = product(theirs, number).astype(bf16)
-                to_mate(step, number).start()
-                keep[step, at, :] = product(ours, number)
-                if waiting:
-                    joined(*waiting.pop())
-                if step:
-                    waiting.append((step, number))
-
-    def settle(phase):
-        for number in range(phase * subs, (phase + 1) * subs):
-            at = within(number)
-            to_mate(0, number).wait_recv()
-            total = keep[0, at, :] + mate_in[0, at, :].astype(f32)
-            for step in range(1, chips):
-                across(step, number).wait_recv()
-                total = total + link_in[step - 1, at, :].astype(f32)
-            out_ref[at, :] = total.astype(bf16)
-
-    attend(0)
-    arrive(0)
-    spread(0)
-    for phase in range(1, phases):
-        attend(phase)
-        settle(phase - 1)
-        arrive(phase)
-        spread(phase)
-    settle(phases - 1)
-    for step in range(chips):
-        for number in range(phases * subs):
-            to_mate(step, number).wait_send()
-            if step:
-                across(step, number).wait_send()
-    for phase in range(phases):
-        for step in range(1, sp_count):
-            away(phase, lax.rem(sp + step, sp_count)).wait_send()
-
-        @pl.when(jnp.logical_not(owner))
-        def _():
-            away(phase, sp).wait_send()
+                spot = odd_spot if source % 2 else even_spot
+
+                @pl.when(jnp.logical_not(stays_here(phase, source, inner, spot)))
+                def _():
+                    away(phase, source, inner, spot).wait_send()
+
+    for step in range(1, tp_count):
+        conv_share(step).wait_send()
+    for part in range(parts):
+        for kind in range(2):
+            for step in range(chips):
+                weights_mate(kind, lax.rem(tp + CORES * step, tp_count), part).wait_send()
+        for step in range(1, chips):
+            weights_across(step, part).wait_send()
+            weights_beside(step, part).wait_send()
 
     @pl.when(owner)
     def _():
@@ -672,7 +701,6 @@
     for number in order:
         to_mate_tokens(number).wait_send()
         for step in range(1, chips):
-            across_tokens(step, number).wait_send()
             token_pass(step, number).wait_send()
 
     @pl.when(sp < sp_count - 1)
@@ -698,8 +726,7 @@
     chips = tp_count // CORES
     targets = sp_count // CORES
     block_rows = rows // tp_count
-    sub = min(64, block_rows // 2)
-    subs = block_rows // sub
+    parts = 4
     links = max(chips - 1, 1)
     bf16 = jnp.bfloat16
     f32 = jnp.float32
@@ -707,14 +734,13 @@
     vmem = pl.BlockSpec(memory_space=VMEM)
     hbm = pl.BlockSpec(memory_space=pl.ANY)
     return pl.pallas_call(
-        functools.partial(layer_kernel, (sp_count, tp_count, heads, head_dim, piece, sub)),
+        functools.partial(layer_kernel, (sp_count, tp_count, heads, head_dim, piece)),
         out_shape=jax.ShapeDtypeStruct((block_rows, out_features), bf16),
         in_specs=[hbm] + [vmem] * 7 + [hbm] * 8,
         out_specs=vmem,
         scratch_shapes=[
             VMEM((6,) + weights[0].shape, bf16),
-            VMEM(weights[6].shape, bf16),
-            VMEM(weights[7].shape, bf16),
+            VMEM((2, tp_count * width, out_features), bf16),
             VMEM((tp_count, rows, features), bf16),
             VMEM((rows, tp_count * features), bf16),
             VMEM((rows, LANES), f32),
@@ -729,20 +755,14 @@
             VMEM((sp_count, slabs, head_dim, LANES), bf16),
             VMEM((sp_count, rows // LANES + 8, LANES), f32),
             VMEM((rows, width), bf16),
+            VMEM((tp_count, block_rows, width), bf16),
             VMEM((phases, sp_count, head_dim, tile), bf16),
-            VMEM((phases, sp_count, head_dim, tile), bf16),
+            VMEM((tp_count * heads, head_dim, block_rows), bf16),
             VMEM((2, 2 * LANES, 2 * tile), bf16),
             VMEM((sp_count, rows // 2, LANES), bf16),
             VMEM((rows, 2 * tile), f32),
             VMEM((rows, 2 * tile), f32),
-            VMEM((width, rows), bf16),
-            VMEM((rows, width), bf16),
-            VMEM((rows, out_features), f32),
-            VMEM((chips, block_rows, out_features), f32),
-            VMEM((chips, block_rows, out_features), bf16),
-            VMEM((chips, block_rows, out_features), bf16),
-            VMEM((links, block_rows, out_features), bf16),
-            VMEM((links, block_rows, out_features), bf16),
+            VMEM((block_rows, out_features), f32),
             dma((8,)), dma, dma((links, chunks)), dma((chunks,)), dma((links, chunks)),
             dma((tp_count, chunks)),
             dma((targets, chunks)), dma((sp_count, chunks)),
@@ -751,8 +771,10 @@
             dma((sp_count, chunks)), dma((sp_count, chunks)),
             dma((sp_count,)), dma((sp_count,)),
             dma((chunks + 1,)), dma((2,)),
-            dma((phases, sp_count)), dma((phases, sp_count)), dma((phases,)),
-            dma((chips, subs)), dma((chips, subs)), dma((links, subs)), dma((links, subs)),
+            dma((phases, sp_count, tile // LANES)), dma((tp_count * heads, block_rows // LANES)),
+            dma((tp_count - 1,)), dma((tp_count,)),
+            dma((2, tp_count, parts)), dma((links, parts)), dma((links, parts)),
+            dma((2, tp_count, parts)),
         ],
         compiler_params=pltpu.CompilerParams(
             collective_id=0, has_side_effects=True, vmem_limit_bytes=63 * 1024 * 1024

time: 112 us -> 94.7 us (0.85)
  the two profiles are of different devices: /device:TPU:24 before, /device:TPU:0 now
where the time goes in v3:
time: 94.7 us; the launch traced here: 93.2 us
  Pallas kernels  90.9 us (96%)
  local copies, waits for them, and re-layouts  2.3 us (2%)
    pallas_call x1, Pallas kernels, layer(): pl.pallas_call(functools.partial(layer_kernel, (sp_count, tp_count, heads...  90.9 us
    unnamed x1, local copies, waits for them, and re-layouts  2.3 us

profile of v3, /device:TPU:0, one launch (start us, length us, event | category | flops | bytes accessed | tf_op | source)
XLA Modules:
  0.0 93.2 jit_solution(7759991470295703775)
XLA Ops:
  0.0 90.9 %shard_map.154 = bf16[256,2048]{1,0:T(8,128)(2,1)} custom-call(bf16[1024,512]{1,0:T(8,128)(2,1)} %tokens_ref.1, f32[1,2048]{1,0:T(1,128)} %bitcast.7, f32[1,64]{1,0:T(1,128)} %bitcast.10, f32[1,64]{1,0:T(1,128)} %bitcast.11, f32[3,256]{1,0:T(4,128)} %taps_ref.1, f32[1,256]{1,0:T(1,128)} %bitcast.8, f32[4,1024]{1,0:T(4,128)} %bitcast.6, f32[1,256]{1,0:T(1,128)} %bitcast.9, ...), custom_call_target="tpu_custom_call" | custom-call | tf_op jit(solution)/shard_map/pallas_call | solution.py:736
  90.9 2.3 %copy.18 = bf16[256,2048]{1,0:T(8,128)(2,1)} copy(bf16[256,2048]{1,0:T(8,128)(2,1)} %shard_map.154) | data formatting | bytes 2097152

commit v4 on v3

--- a/solution.py
+++ b/solution.py
@@ -295,15 +295,6 @@
                     ] = turned[inner * head_dim : (inner + 1) * head_dim]
         slab_copies(2 * number, True)
 
-    for index in (1, 2, 0):
-        loads[index].wait()
-    for number in order:
-        take_tokens(number)
-        send_keys(number)
-        send_queries(number)
-    for number in order:
-        slab_copies(2 * number + 1, True)
-
     def part_of(kind, source, part):
         at = pl.multiple_of(source * width + part * part_rows, part_rows)
         return out_weights.at[kind, pl.ds(at, part_rows)]
@@ -318,6 +309,12 @@
             (sp, lax.rem(tp + CORES * step, tp_count)),
         )
 
+    def weights_last(step):
+        return weights_to(
+            1 - parity, tp, parts - 1, out_cross.at[step - 1, parts],
+            (sp, lax.rem(tp + CORES * step, tp_count)),
+        )
+
     def weights_beside(step, part):
         source = lax.rem(tp + CORES * step, tp_count)
         return weights_to(parity, source, part, out_side.at[step - 1, part], (beside, tp))
@@ -329,7 +326,8 @@
         for step in range(1, chips):
             source = lax.rem(tp + CORES * step, tp_count)
             weights_mate(parity, source, part).wait_recv()
-            weights_beside(step, part).start()
+            if part < parts - 1:
+                weights_beside(step, part).start()
             weights_mate(parity, source, part).start()
 
     def from_beside(part):
@@ -338,13 +336,15 @@
             weights_mate(1 - parity, source, part).wait_recv()
             weights_mate(1 - parity, source, part).start()
 
-    loads[6].wait()
-    loads[7].wait()
-    for step in range(1, chips):
-        for number in order:
-            across_tokens(step, number).wait_send()
-        for part in range(parts):
-            weights_across(step, part).start()
+    def start_weights():
+        loads[6].wait()
+        loads[7].wait()
+        for step in range(1, chips):
+            for number in order:
+                across_tokens(step, number).wait_send()
+            for part in range(parts):
+                weights_across(step, part).start()
+            weights_last(step).start()
 
     sources = [lax.rem(sp + step, sp_count) for step in range(sp_count)]
 
@@ -359,23 +359,6 @@
             side_in.at[source], side_in.at[source], side_psem.at[source], side_prsem.at[source],
             (sp, mate),
         )
-
-    @pl.when(owner)
-    def _():
-        for step, source in enumerate(sources):
-            if step == 0:
-                kept_side(0).wait()
-            else:
-                mesh_copy(
-                    side_send.at[0], side_in.at[source], side_ssem.at[0], side_rsem.at[source],
-                    (sp, mate),
-                ).wait_recv()
-            side_pass(source).start()
-
-    @pl.when(jnp.logical_not(owner))
-    def _():
-        for source in sources:
-            side_pass(source).wait_recv()
 
     def forward(number):
         @pl.when(owner)
@@ -390,9 +373,6 @@
                     ).wait_recv()
                 kv_pass(source, number).start()
 
-    gain_tile = jnp.broadcast_to(side_in[0, rows // LANES : rows // LANES + 1, :], (LANES, LANES))
-    gain = gain_tile.T[:head_dim, 0:1]
-
     def pieces_of(values):
         high = values.astype(bf16).astype(f32)
         middle = (values - high).astype(bf16).astype(f32)
@@ -411,9 +391,6 @@
             )
         return 0
 
-    forward(order[0])
-    lax.fori_loop(0, sp_count, gate_columns, 0)
-
     def conv_inputs(number):
         here = block(number)
         outer[here, :] = project(number, 3)
@@ -424,9 +401,36 @@
     edge = mesh_copy(
         edge_send, edge_recv, edge_sem.at[0], edge_sem.at[1], (lax.rem(sp + 1, sp_count), tp)
     )
-    for index in (3, 4, 5):
+    def take_sides():
+        @pl.when(owner)
+        def _():
+            for step, source in enumerate(sources):
+                if step == 0:
+                    kept_side(0).wait()
+                else:
+                    mesh_copy(
+                        side_send.at[0], side_in.at[source], side_ssem.at[0], side_rsem.at[source],
+                        (sp, mate),
+                    ).wait_recv()
+                side_pass(source).start()
+
+        @pl.when(jnp.logical_not(owner))
+        def _():
+            for source in sources:
+                side_pass(source).wait_recv()
+
+        lax.fori_loop(0, sp_count, gate_columns, 0)
+
+    for index in (1, 2, 0, 3, 4, 5):
         loads[index].wait()
     for position, number in enumerate(order):
+        take_tokens(number)
+        send_keys(number)
+        send_queries(number)
+        if position == chunks - 1:
+            for other in order:
+                slab_copies(2 * other + 1, True)
+            start_weights()
         gated = conv_inputs(number)
         if position == 0:
             edge_send[...] = gated[chunk - 16 :, :]
@@ -435,8 +439,12 @@
             def _():
                 edge.start()
 
-        elif position < chunks - 1:
-            forward(number)
+            take_sides()
+        if position > 1:
+            forward(order[position - 2])
+    gain_tile = jnp.broadcast_to(side_in[0, rows // LANES : rows // LANES + 1, :], (LANES, LANES))
+    gain = gain_tile.T[:head_dim, 0:1]
+
 
     @pl.when(sp > 0)
     def _():
@@ -465,7 +473,10 @@
         conv_share(step).start()
     own_rows = pl.ds(pl.multiple_of(tp * block_rows, block_rows), block_rows)
     conv_in[tp, :, :] = conv_mixed[own_rows, :]
+    forward(order[-2])
+    from_across(0)
     forward(order[-1])
+    from_across(1)
 
     @pl.when(jnp.logical_not(owner))
     def _():
@@ -476,8 +487,6 @@
     for kind in range(2):
         for part in range(parts):
             weights_mate(kind, tp, part).start()
-    for part in range(parts // 2):
-        from_across(part)
 
     def place_of(phase, inner, spot):
         begin = (inner * phases + phase) * half
@@ -611,20 +620,25 @@
 
         if phase == 0:
             scores_b[...] = jnp.zeros_like(scores_b)
-        state, top, last = lax.fori_loop(
-            0, sp_count // 2, pair_of_sources, (empty, jnp.zeros((1, both_tiles), f32), 0)
-        )
+        carried = (empty, jnp.zeros((1, both_tiles), f32), 0)
+        pairs = sp_count // 2
+        carried = lax.fori_loop(0, pairs - 1, pair_of_sources, carried)
+        hook(phase)
+        state, top, last = lax.fori_loop(pairs - 1, pairs, pair_of_sources, carried)
         state, _ = advance(last, scores_b, top, state, None, None)
         finish(phase, sp_count - 2, state[1][:, :tile], even_spot)
         finish(phase, sp_count - 1, state[1][:, tile:], odd_spot)
 
+    def hook(phase):
+        if phase == 0:
+            from_across(2)
+            from_across(3)
+        if phase == phases - 1:
+            for part in range(parts):
+                from_beside(part)
+
     for phase in range(phases):
         attend(phase)
-        if phase == 0:
-            for part in range(parts // 2, parts):
-                from_across(part)
-    for part in range(parts):
-        from_beside(part)
     for step in range(1, tp_count):
         source = lax.rem(tp + step, tp_count)
         mesh_copy(
@@ -678,7 +692,10 @@
                 weights_mate(kind, lax.rem(tp + CORES * step, tp_count), part).wait_send()
         for step in range(1, chips):
             weights_across(step, part).wait_send()
-            weights_beside(step, part).wait_send()
+            if part < parts - 1:
+                weights_beside(step, part).wait_send()
+            else:
+                weights_last(step).wait_send()
 
     @pl.when(owner)
     def _():
@@ -773,7 +790,7 @@
             dma((chunks + 1,)), dma((2,)),
             dma((phases, sp_count, tile // LANES)), dma((tp_count * heads, block_rows // LANES)),
             dma((tp_count - 1,)), dma((tp_count,)),
-            dma((2, tp_count, parts)), dma((links, parts)), dma((links, parts)),
+            dma((2, tp_count, parts)), dma((links, parts + 1)), dma((links, parts)),
             dma((2, tp_count, parts)),
         ],
         compiler_params=pltpu.CompilerParams(

time: 94.7 us -> 92.7 us (0.979); the launches traced: 93.2 us -> 92.5 us
  no operation moved by 1% of the time
where the time goes in v4:
time: 92.7 us; the launch traced here: 92.5 us
  Pallas kernels  90.2 us (97%)
  local copies, waits for them, and re-layouts  2.3 us (2%)
    pallas_call x1, Pallas kernels, layer(): pl.pallas_call(functools.partial(layer_kernel, (sp_count, tp_count, heads...  90.2 us
    unnamed x1, local copies, waits for them, and re-layouts  2.3 us

profile of v4, /device:TPU:0, one launch (start us, length us, event | category | flops | bytes accessed | tf_op | source)
XLA Modules:
  0.0 92.5 jit_solution(13635459623643733320)
XLA Ops:
  0.0 90.2 %shard_map.154 = bf16[256,2048]{1,0:T(8,128)(2,1)} custom-call(bf16[1024,512]{1,0:T(8,128)(2,1)} %tokens_ref.1, f32[1,2048]{1,0:T(1,128)} %bitcast.7, f32[1,64]{1,0:T(1,128)} %bitcast.10, f32[1,64]{1,0:T(1,128)} %bitcast.11, f32[3,256]{1,0:T(4,128)} %taps_ref.1, f32[1,256]{1,0:T(1,128)} %bitcast.8, f32[4,1024]{1,0:T(4,128)} %bitcast.6, f32[1,256]{1,0:T(1,128)} %bitcast.9, ...), custom_call_target="tpu_custom_call" | custom-call | tf_op jit(solution)/shard_map/pallas_call | solution.py:753
  90.2 2.3 %copy.18 = bf16[256,2048]{1,0:T(8,128)(2,1)} copy(bf16[256,2048]{1,0:T(8,128)(2,1)} %shard_map.154) | data formatting | bytes 2097152

commit v5 on v4

--- a/solution.py
+++ b/solution.py
@@ -597,16 +597,23 @@
             jnp.full((1, both_tiles), -1e30, f32), jnp.zeros((head_dim, both_tiles), f32)
         )
 
-        def pair_of_sources(pair, carried):
+        pairs = sp_count // 2
+
+        def pair_at(index):
+            return index + (index == pairs - 2) * 1 - (index == pairs - 1) * 1
+
+        def pair_of_sources(index, carried):
             state, top, last = carried
+            pair = pair_at(index)
+            before = 2 * pair_at(index - 1)
             even, odd = 2 * pair, 2 * pair + 1
             set_queries(phase, even, odd)
             state, top = advance(last, scores_b, top, state, even, scores_a, even_limit)
 
-            @pl.when(pair > 0)
+            @pl.when(index > 0)
             def _():
-                finish(phase, even - 2, state[1][:, :tile], even_spot)
-                finish(phase, odd - 2, state[1][:, tile:], odd_spot)
+                finish(phase, before, state[1][:, :tile], even_spot)
+                finish(phase, before + 1, state[1][:, tile:], odd_spot)
 
             state, top = advance(even, scores_a, top, empty, odd, scores_b, odd_limit)
 
@@ -621,13 +628,12 @@
         if phase == 0:
             scores_b[...] = jnp.zeros_like(scores_b)
         carried = (empty, jnp.zeros((1, both_tiles), f32), 0)
-        pairs = sp_count // 2
         carried = lax.fori_loop(0, pairs - 1, pair_of_sources, carried)
         hook(phase)
         state, top, last = lax.fori_loop(pairs - 1, pairs, pair_of_sources, carried)
         state, _ = advance(last, scores_b, top, state, None, None)
-        finish(phase, sp_count - 2, state[1][:, :tile], even_spot)
-        finish(phase, sp_count - 1, state[1][:, tile:], odd_spot)
+        finish(phase, sp_count - 4, state[1][:, :tile], even_spot)
+        finish(phase, sp_count - 3, state[1][:, tile:], odd_spot)
 
     def hook(phase):
         if phase == 0:

time: 92.7 us -> 91.4 us (0.986)
  Pallas kernels: 90.2 us -> 88.9 us
    pallas_call x1, Pallas kernels: 90.2 us -> 88.9 us  [layer(): pl.pallas_call(functools.partial(layer_kernel, (sp_count, tp_count, heads...]
where the time goes in v5:
time: 91.4 us; the launch traced here: 91.2 us
  Pallas kernels  88.9 us (97%)
  local copies, waits for them, and re-layouts  2.3 us (3%)
    pallas_call x1, Pallas kernels, layer(): pl.pallas_call(functools.partial(layer_kernel, (sp_count, tp_count, heads...  88.9 us
    unnamed x1, local copies, waits for them, and re-layouts  2.3 us

profile of v5, /device:TPU:0, one launch (start us, length us, event | category | flops | bytes accessed | tf_op | source)
XLA Modules:
  0.0 91.2 jit_solution(1516559387757170649)
XLA Ops:
  0.0 88.9 %shard_map.154 = bf16[256,2048]{1,0:T(8,128)(2,1)} custom-call(bf16[1024,512]{1,0:T(8,128)(2,1)} %tokens_ref.1, f32[1,2048]{1,0:T(1,128)} %bitcast.7, f32[1,64]{1,0:T(1,128)} %bitcast.10, f32[1,64]{1,0:T(1,128)} %bitcast.11, f32[3,256]{1,0:T(4,128)} %taps_ref.1, f32[1,256]{1,0:T(1,128)} %bitcast.8, f32[4,1024]{1,0:T(4,128)} %bitcast.6, f32[1,256]{1,0:T(1,128)} %bitcast.9, ...), custom_call_target="tpu_custom_call" | custom-call | tf_op jit(solution)/shard_map/pallas_call | solution.py:759
  88.9 2.3 %copy.18 = bf16[256,2048]{1,0:T(8,128)(2,1)} copy(bf16[256,2048]{1,0:T(8,128)(2,1)} %shard_map.154) | data formatting | bytes 2097152
